TPU v7x, 512 devices: a whole 4x8x8 slice. The times are simulated.
512 devices in a mesh: tp: 32 (over z, x), dp: 16 (over y, core).
Axes of the slice: x: 4, y: 8, z: 8, core: 2. Of those that a mesh axis runs over, the one named last changes fastest.
Arguments:
- tokens: bfloat16 [256, 4096], P(None, 'dp'), may hold values from -6 to 6
- recurrent_state: float32 [2, 256, 262144], P(None, 'dp', 'tp'), may hold values from -24 to 24
- pre_gain: float32 [2, 4096], P(None, 'dp'), may hold values from 0.1 to 1.9
- w_query: bfloat16 [2, 4096, 2048], P(None, 'dp', 'tp'), may hold values from -0.09375 to 0.09375
- w_key: bfloat16 [2, 4096, 2048], P(None, 'dp', 'tp'), may hold values from -0.09375 to 0.09375
- w_value: bfloat16 [2, 4096, 4096], P(None, 'dp', 'tp'), may hold values from -0.09375 to 0.09375
- w_gate: bfloat16 [2, 4096, 4096], P(None, 'dp', 'tp'), may hold values from -0.09375 to 0.09375
- w_decay: bfloat16 [2, 4096, 2048], P(None, 'dp', 'tp'), may hold values from -1 to 1
- decay_bias: float32 [2, 2048], P(None, 'tp'), may hold values from -5 to 3
- head_gain: float32 [2, 128], replicated, may hold values from 0.1 to 1.9
- w_out: bfloat16 [2, 4096, 4096], P(None, 'tp', 'dp'), may hold values from -0.09375 to 0.09375
- post_gain: float32 [2, 4096], P(None, 'dp'), may hold values from 0.1 to 1.9
Outputs:
- hidden_out: bfloat16 [256, 4096], P(None, 'dp')
- state_out: float32 [2, 256, 262144], P(None, 'dp', 'tp')
All inputs are finite; a program needn't handle non-finite values.
Results may differ from a plain program's by a relative error of at most 0.015.
Values may be sent and summed in bfloat16 or wider, within the bound.
A program may use at most 64 MiB of HBM per device.

v0:
```python
import jax
import jax.numpy as jnp
from jax import lax
from jax.sharding import PartitionSpec as P

D = 4096
KEY = 64
VAL = 128


epsilon = 1e-06


def split_up(array, dim, size):
    before, after = (array.shape[:dim], array.shape[dim + 1 :])
    return jnp.moveaxis(array.reshape(*before, size, -1, *after), dim, 0)


def summed_on_arrival(array, axis, dim):
    size = lax.axis_size(axis)
    tiles = lax.all_to_all(split_up(array, dim, size), axis, 0, 0, tiled=True)
    return jnp.sum(tiles, axis=0)


def sent_to_all(array, axis):
    size = lax.axis_size(axis)
    return lax.all_to_all(
        jnp.broadcast_to(array[None], (size, *array.shape)), axis, 0, 0, tiled=True
    )


def laid_out(tiles, dim):
    tiles = jnp.moveaxis(tiles, 0, dim)
    shape = tiles.shape
    return tiles.reshape(*shape[:dim], shape[dim] * shape[dim + 1], *shape[dim + 2 :])


def gathered_copies(array, axis, dim):
    tiles = sent_to_all(array, axis)
    return laid_out(tiles, dim)


def sum_at_owner(array, axis, dim):
    tiles = split_up(array, dim, lax.axis_size(axis))
    arrived = lax.all_to_all(tiles, axis, split_axis=0, concat_axis=0, tiled=True)
    return arrived.astype(jnp.float32).sum(axis=0)


def over_copies(array, axis):
    return sent_to_all(array, axis).sum(axis=0)


def local(
    tokens,
    recurrent_state,
    pre_gain,
    w_query,
    w_key,
    w_value,
    w_gate,
    w_decay,
    decay_bias,
    head_gain,
    w_out,
    post_gain,
):
    column_count = lax.axis_size("tp")
    column_rank = lax.axis_index("tp")
    seq_all = tokens.shape[0]
    local_seqs = recurrent_state.shape[1]
    value_cols = recurrent_state.shape[2] // KEY
    heads_here = value_cols // VAL
    highest = lax.Precision.HIGHEST
    spread = (
        jnp.arange(value_cols, dtype=jnp.int32)[None, :] // VAL
        == jnp.arange(heads_here, dtype=jnp.int32)[:, None]
    ).astype(jnp.float32)

    def spread_heads(vectors):
        shaped = vectors.astype(jnp.float32).reshape(local_seqs, heads_here, KEY)
        return jnp.einsum("bhk,hc->bck", shaped, spread, precision=highest)

    residual = tokens
    new_states = []
    for section_index in range(2):
        wide_float = residual.astype(jnp.float32)
        squares_part = jnp.sum(wide_float * wide_float, axis=1)
        normed = (wide_float * pre_gain[section_index]).astype(jnp.bfloat16)
        partials = tuple(
            (
                jnp.dot(normed, weights[section_index], preferred_element_type=jnp.float32)
                for weights in (w_query, w_key, w_value, w_gate, w_decay)
            )
        )
        summed = jax.tree.map(
            lambda part: summed_on_arrival(part, "dp", 0), partials + (squares_part,)
        )
        projected = summed[:5]
        own_squares = summed[5]
        row_scale = lax.rsqrt(own_squares / D + epsilon)[:, None]
        query_part = (projected[0] * row_scale).astype(jnp.bfloat16)
        key_part = (projected[1] * row_scale).astype(jnp.bfloat16)
        values_own = projected[2] * row_scale
        gate_pre = projected[3] * row_scale
        log_decay = jax.nn.log_sigmoid(projected[4] * row_scale + decay_bias[section_index]) / 16.0
        query_cols = spread_heads(query_part)
        key_cols = spread_heads(key_part)
        decay_cols = jnp.exp(spread_heads(log_decay))
        old_state = recurrent_state[section_index].reshape(local_seqs, value_cols, KEY)
        new_state = decay_cols * old_state + key_cols * values_own[:, :, None]
        readout = jnp.sum(query_cols * new_state, axis=2) * KEY ** (-0.5)
        head_mean = jnp.mean(
            (readout * readout).reshape(local_seqs, heads_here, VAL), axis=2, keepdims=True
        )
        scaled = (
            readout.reshape(local_seqs, heads_here, VAL)
            * lax.rsqrt(head_mean + epsilon)
            * head_gain[section_index]
        )
        mixed = (scaled.reshape(local_seqs, value_cols) * jax.nn.silu(gate_pre)).astype(
            jnp.bfloat16
        )
        out_weight = w_out[section_index]
        gathered = gathered_copies(mixed, "dp", 0)
        share_rows = seq_all // column_count
        out_rows = sum_at_owner(
            jnp.dot(gathered, out_weight, preferred_element_type=jnp.float32).astype(jnp.bfloat16),
            "tp",
            0,
        )
        out_squares = over_copies(jnp.sum(out_rows * out_rows, axis=1), "dp")
        own_rows = lax.dynamic_slice_in_dim(
            residual, column_rank * share_rows, share_rows, 0
        ).astype(jnp.float32)
        updated = (
            own_rows
            + out_rows * lax.rsqrt(out_squares / D + epsilon)[:, None] * post_gain[section_index]
        ).astype(jnp.bfloat16)
        residual = gathered_copies(updated, "tp", 0)
        new_states.append(new_state.reshape(local_seqs, value_cols * KEY))
    return (residual, jnp.stack(new_states))


def solution(mesh):
    in_specs = (
        P(None, "dp"),
        P(None, "dp", "tp"),
        P(None, "dp"),
        P(None, "dp", "tp"),
        P(None, "dp", "tp"),
        P(None, "dp", "tp"),
        P(None, "dp", "tp"),
        P(None, "dp", "tp"),
        P(None, "tp"),
        P(),
        P(None, "tp", "dp"),
        P(None, "dp"),
    )
    out_specs = (P(None, "dp"), P(None, "dp", "tp"))
    return jax.shard_map(local, mesh=mesh, in_specs=in_specs, out_specs=out_specs, check_vma=False)
```

profile of v0, /device:TPU:1, one launch (start us, length us, event | category | flops | bytes accessed | tf_op | source)
XLA Modules:
  0.0 265.5 jit_solution(10752713642527964072)
XLA Ops:
  0.6 0.8 fusion.71
  1.4 1.0 fusion.7
  2.5 0.7 all_to_all.69
  3.1 10.1 %all-to-all-start.1 = ((f32[16,1,16]{2,1,0:T(1,128)}), f32[16,1,16]{2,1,0:T(1,128)S(1)}, u32[]{:S(2)}, u32[]{:S(2)}) async-start(f32[16,1,16]{2,1,0:T(1,128)} %all_to_all.69), calls=%async_computation.1 | async-start | bytes 16384 | tf_op jit(solution)/shard_map/all_to_all | solution.py:21
  13.2 1.7 fusion.16
  14.9 0.9 fusion.32
  15.8 0.9 fusion.34
  16.9 0.8 copy-done.7
  17.8 0.8 reshape.815
  18.5 0.7 reshape.817
  19.3 0.7 reshape.819
  20.3 7.0 %all-to-all-start.3 = ((f32[16,1,1024]{2,1,0:T(1,128)}), f32[16,1,1024]{2,1,0:T(1,128)S(1)}, u32[]{:S(2)}, u32[]{:S(2)}) async-start(f32[16,1,1024]{2,1,0:T(1,128)} %reshape.815), calls=%async_computation.3 | async-start | bytes 131072 | tf_op jit(solution)/shard_map/all_to_all | solution.py:21
  27.3 0.8 fusion.18
  28.1 6.9 %all-to-all-done.3 = f32[16,1,1024]{2,1,0:T(1,128)S(1)} async-done(((f32[16,1,1024]{2,1,0:T(1,128)}), f32[16,1,1024]{2,1,0:T(1,128)S(1)}, u32[]{:S(2)}, u32[]{:S(2)}) %all-to-all-start.3) | async-done | bytes 65568 | tf_op jit(solution)/shard_map/all_to_all | solution.py:21
  35.1 3.4 %all-to-all-start = ((f32[16,1,1024]{2,1,0:T(1,128)}), f32[16,1,1024]{2,1,0:T(1,128)S(1)}, u32[]{:S(2)}, u32[]{:S(2)}) async-start(f32[16,1,1024]{2,1,0:T(1,128)} %reshape.819), calls=%async_computation | async-start | bytes 131072 | tf_op jit(solution)/shard_map/all_to_all | solution.py:21
  38.5 7.8 %all-to-all-done = f32[16,1,1024]{2,1,0:T(1,128)S(1)} async-done(((f32[16,1,1024]{2,1,0:T(1,128)}), f32[16,1,1024]{2,1,0:T(1,128)S(1)}, u32[]{:S(2)}, u32[]{:S(2)}) %all-to-all-start) | async-done | bytes 65568 | tf_op jit(solution)/shard_map/all_to_all | solution.py:21
  46.3 3.4 %all-to-all-start.2 = ((f32[16,1,1024]{2,1,0:T(1,128)}), f32[16,1,1024]{2,1,0:T(1,128)S(1)}, u32[]{:S(2)}, u32[]{:S(2)}) async-start(f32[16,1,1024]{2,1,0:T(1,128)} %reshape.817), calls=%async_computation.2 | async-start | bytes 131072 | tf_op jit(solution)/shard_map/all_to_all | solution.py:21
  50.7 6.8 %all-to-all-done.2 = f32[16,1,1024]{2,1,0:T(1,128)S(1)} async-done(((f32[16,1,1024]{2,1,0:T(1,128)}), f32[16,1,1024]{2,1,0:T(1,128)S(1)}, u32[]{:S(2)}, u32[]{:S(2)}) %all-to-all-start.2) | async-done | bytes 65568 | tf_op jit(solution)/shard_map/all_to_all | solution.py:21
  57.6 3.5 %all-to-all-start.4 = ((f32[16,16,128]{2,1,0:T(8,128)}), f32[16,16,128]{2,1,0:T(8,128)S(1)}, u32[]{:S(2)}, u32[]{:S(2)}) async-start(f32[16,16,128]{2,1,0:T(8,128)} %fusion.18), calls=%async_computation.4 | async-start | bytes 262144 | tf_op jit(solution)/shard_map/all_to_all | solution.py:21
  61.6 0.8 reduce.8
  62.6 0.8 reduce.7
  63.5 0.8 reduce.9
  64.6 5.6 %all-to-all-done.4 = f32[16,16,128]{2,1,0:T(8,128)S(1)} async-done(((f32[16,16,128]{2,1,0:T(8,128)}), f32[16,16,128]{2,1,0:T(8,128)S(1)}, u32[]{:S(2)}, u32[]{:S(2)}) %all-to-all-start.4) | async-done | bytes 131104 | tf_op jit(solution)/shard_map/all_to_all | solution.py:21
  70.2 3.4 %all-to-all-start.5 = ((f32[16,16,128]{2,1,0:T(8,128)}), f32[16,16,128]{2,1,0:T(8,128)S(1)}, u32[]{:S(2)}, u32[]{:S(2)}) async-start(f32[16,16,128]{2,1,0:T(8,128)} %fusion.16), calls=%async_computation.5 | async-start | bytes 262144 | tf_op jit(solution)/shard_map/all_to_all | solution.py:21
  73.7 0.7 fusion.5
  74.6 7.5 %all-to-all-done.5 = f32[16,16,128]{2,1,0:T(8,128)S(1)} async-done(((f32[16,16,128]{2,1,0:T(8,128)}), f32[16,16,128]{2,1,0:T(8,128)S(1)}, u32[]{:S(2)}, u32[]{:S(2)}) %all-to-all-start.5) | async-done | bytes 131104 | tf_op jit(solution)/shard_map/all_to_all | solution.py:21
  82.2 10.5 %all_to_all.110 = bf16[16,16,128]{2,1,0:T(8,128)(2,1)S(1)} all-to-all(bf16[16,16,128]{2,1,0:T(8,128)(2,1)S(1)} %broadcast_in_dim.12), channel_id=1, replica_groups=mesh['tp'=32,'dp'=16] {'dp'}, dimensions={0} | all-to-all | bytes 131072 | tf_op jit(solution)/shard_map/all_to_all | solution.py:27
  92.8 21.0 %all_to_all.111 = bf16[32,8,256]{2,1,0:T(8,128)(2,1)S(1)} all-to-all(bf16[32,8,256]{2,1,0:T(8,128)(2,1)S(1)} %fusion), channel_id=1, replica_groups=mesh['tp'=32,'dp'=16] {'tp'}, dimensions={0} | all-to-all | bytes 262144 | tf_op jit(solution)/shard_map/all_to_all | solution.py:45
  114.6 4.9 %all-to-all-start.8 = ((f32[16,1,8]{2,1,0:T(1,128)}), f32[16,1,8]{2,1,0:T(1,128)S(1)}, u32[]{:S(2)}, u32[]{:S(2)}) async-start(f32[16,1,8]{2,1,0:T(1,128)} %broadcast_in_dim.13), calls=%async_computation.8 | async-start | bytes 16384 | tf_op jit(solution)/shard_map/all_to_all | solution.py:27
  120.1 6.5 %all-to-all-done.8 = f32[16,1,8]{2,1,0:T(1,128)S(1)} async-done(((f32[16,1,8]{2,1,0:T(1,128)}), f32[16,1,8]{2,1,0:T(1,128)S(1)}, u32[]{:S(2)}, u32[]{:S(2)}) %all-to-all-start.8) | async-done | bytes 544 | tf_op jit(solution)/shard_map/all_to_all | solution.py:27
  126.6 0.8 add_convert_fusion.1
  128.0 3.9 %all-to-all-start.9 = ((bf16[32,8,256]{2,1,0:T(8,128)(2,1)}), bf16[32,8,256]{2,1,0:T(8,128)(2,1)S(1)}, u32[]{:S(2)}, u32[]{:S(2)}) async-start(bf16[32,8,256]{2,1,0:T(8,128)(2,1)} %broadcast_in_dim.14), calls=%async_computation.9 | async-start | bytes 262144 | tf_op jit(solution)/shard_map/all_to_all | solution.py:27
  132.3 9.0 %all-to-all-done.9 = bf16[32,8,256]{2,1,0:T(8,128)(2,1)S(1)} async-done(((bf16[32,8,256]{2,1,0:T(8,128)(2,1)}), bf16[32,8,256]{2,1,0:T(8,128)(2,1)S(1)}, u32[]{:S(2)}, u32[]{:S(2)}) %all-to-all-start.9) | async-done | bytes 131104 | tf_op jit(solution)/shard_map/all_to_all | solution.py:27
  141.4 0.7 all_to_all.80
  142.1 5.3 %all-to-all-start.11 = ((f32[16,1,16]{2,1,0:T(1,128)}), f32[16,1,16]{2,1,0:T(1,128)S(1)}, u32[]{:S(2)}, u32[]{:S(2)}) async-start(f32[16,1,16]{2,1,0:T(1,128)} %bitcast.35), calls=%async_computation.11 | async-start | bytes 16384 | tf_op jit(solution)/shard_map/all_to_all | solution.py:21
  147.6 0.7 copy-done.6
  148.4 0.8 reshape.821
  149.2 0.7 reshape.823
  150.0 4.5 %all-to-all-done.11 = f32[16,1,16]{2,1,0:T(1,128)S(1)} async-done(((f32[16,1,16]{2,1,0:T(1,128)}), f32[16,1,16]{2,1,0:T(1,128)S(1)}, u32[]{:S(2)}, u32[]{:S(2)}) %all-to-all-start.11) | async-done | bytes 1056 | tf_op jit(solution)/shard_map/all_to_all | solution.py:21
  154.4 4.0 %all-to-all-start.13 = ((f32[16,1,1024]{2,1,0:T(1,128)}), f32[16,1,1024]{2,1,0:T(1,128)S(1)}, u32[]{:S(2)}, u32[]{:S(2)}) async-start(f32[16,1,1024]{2,1,0:T(1,128)} %reshape.821), calls=%async_computation.13 | async-start | bytes 131072 | tf_op jit(solution)/shard_map/all_to_all | solution.py:21
  158.6 0.8 reshape.825
  159.3 6.9 %all-to-all-done.13 = f32[16,1,1024]{2,1,0:T(1,128)S(1)} async-done(((f32[16,1,1024]{2,1,0:T(1,128)}), f32[16,1,1024]{2,1,0:T(1,128)S(1)}, u32[]{:S(2)}, u32[]{:S(2)}) %all-to-all-start.13) | async-done | bytes 65568 | tf_op jit(solution)/shard_map/all_to_all | solution.py:21
  166.2 3.5 %all-to-all-start.10 = ((f32[16,1,1024]{2,1,0:T(1,128)}), f32[16,1,1024]{2,1,0:T(1,128)S(1)}, u32[]{:S(2)}, u32[]{:S(2)}) async-start(f32[16,1,1024]{2,1,0:T(1,128)} %reshape.825), calls=%async_computation.10 | async-start | bytes 131072 | tf_op jit(solution)/shard_map/all_to_all | solution.py:21
  169.7 0.8 fusion.11
  170.5 7.0 %all-to-all-done.10 = f32[16,1,1024]{2,1,0:T(1,128)S(1)} async-done(((f32[16,1,1024]{2,1,0:T(1,128)}), f32[16,1,1024]{2,1,0:T(1,128)S(1)}, u32[]{:S(2)}, u32[]{:S(2)}) %all-to-all-start.10) | async-done | bytes 65568 | tf_op jit(solution)/shard_map/all_to_all | solution.py:21
  177.5 3.4 %all-to-all-start.12 = ((f32[16,1,1024]{2,1,0:T(1,128)}), f32[16,1,1024]{2,1,0:T(1,128)S(1)}, u32[]{:S(2)}, u32[]{:S(2)}) async-start(f32[16,1,1024]{2,1,0:T(1,128)} %reshape.823), calls=%async_computation.12 | async-start | bytes 131072 | tf_op jit(solution)/shard_map/all_to_all | solution.py:21
  180.9 0.8 fusion.13
  181.8 7.0 %all-to-all-done.12 = f32[16,1,1024]{2,1,0:T(1,128)S(1)} async-done(((f32[16,1,1024]{2,1,0:T(1,128)}), f32[16,1,1024]{2,1,0:T(1,128)S(1)}, u32[]{:S(2)}, u32[]{:S(2)}) %all-to-all-start.12) | async-done | bytes 65568 | tf_op jit(solution)/shard_map/all_to_all | solution.py:21
  188.8 3.5 %all-to-all-start.14 = ((f32[16,16,128]{2,1,0:T(8,128)}), f32[16,16,128]{2,1,0:T(8,128)S(1)}, u32[]{:S(2)}, u32[]{:S(2)}) async-start(f32[16,16,128]{2,1,0:T(8,128)} %fusion.13), calls=%async_computation.14 | async-start | bytes 262144 | tf_op jit(solution)/shard_map/all_to_all | solution.py:21
  192.3 0.8 reduce.11
  193.2 0.8 reduce.10
  194.2 0.8 reduce.12
  195.1 0.7 fusion.49
  195.8 5.6 %all-to-all-done.14 = f32[16,16,128]{2,1,0:T(8,128)S(1)} async-done(((f32[16,16,128]{2,1,0:T(8,128)}), f32[16,16,128]{2,1,0:T(8,128)S(1)}, u32[]{:S(2)}, u32[]{:S(2)}) %all-to-all-start.14) | async-done | bytes 131104 | tf_op jit(solution)/shard_map/all_to_all | solution.py:21
  201.4 3.4 %all-to-all-start.15 = ((f32[16,16,128]{2,1,0:T(8,128)}), f32[16,16,128]{2,1,0:T(8,128)S(1)}, u32[]{:S(2)}, u32[]{:S(2)}) async-start(f32[16,16,128]{2,1,0:T(8,128)} %fusion.11), calls=%async_computation.15 | async-start | bytes 262144 | tf_op jit(solution)/shard_map/all_to_all | solution.py:21
  205.6 0.7 fusion.3
  206.4 6.9 %all-to-all-done.15 = f32[16,16,128]{2,1,0:T(8,128)S(1)} async-done(((f32[16,16,128]{2,1,0:T(8,128)}), f32[16,16,128]{2,1,0:T(8,128)S(1)}, u32[]{:S(2)}, u32[]{:S(2)}) %all-to-all-start.15) | async-done | bytes 131104 | tf_op jit(solution)/shard_map/all_to_all | solution.py:21
  214.0 10.5 %all_to_all.112 = bf16[16,16,128]{2,1,0:T(8,128)(2,1)S(1)} all-to-all(bf16[16,16,128]{2,1,0:T(8,128)(2,1)S(1)} %broadcast_in_dim.15), channel_id=1, replica_groups=mesh['tp'=32,'dp'=16] {'dp'}, dimensions={0} | all-to-all | bytes 131072 | tf_op jit(solution)/shard_map/all_to_all | solution.py:27
  224.6 12.8 %all_to_all.113 = bf16[32,8,256]{2,1,0:T(8,128)(2,1)S(1)} all-to-all(bf16[32,8,256]{2,1,0:T(8,128)(2,1)S(1)} %fusion.1), channel_id=1, replica_groups=mesh['tp'=32,'dp'=16] {'tp'}, dimensions={0} | all-to-all | bytes 262144 | tf_op jit(solution)/shard_map/all_to_all | solution.py:45
  238.2 4.9 %all-to-all-start.18 = ((f32[16,1,8]{2,1,0:T(1,128)}), f32[16,1,8]{2,1,0:T(1,128)S(1)}, u32[]{:S(2)}, u32[]{:S(2)}) async-start(f32[16,1,8]{2,1,0:T(1,128)} %broadcast_in_dim.16), calls=%async_computation.18 | async-start | bytes 16384 | tf_op jit(solution)/shard_map/all_to_all | solution.py:27
  243.8 6.3 %all-to-all-done.18 = f32[16,1,8]{2,1,0:T(1,128)S(1)} async-done(((f32[16,1,8]{2,1,0:T(1,128)}), f32[16,1,8]{2,1,0:T(1,128)S(1)}, u32[]{:S(2)}, u32[]{:S(2)}) %all-to-all-start.18) | async-done | bytes 544 | tf_op jit(solution)/shard_map/all_to_all | solution.py:27
  251.6 3.9 %all-to-all-start.19 = ((bf16[32,8,256]{2,1,0:T(8,128)(2,1)}), bf16[32,8,256]{2,1,0:T(8,128)(2,1)S(1)}, u32[]{:S(2)}, u32[]{:S(2)}) async-start(bf16[32,8,256]{2,1,0:T(8,128)(2,1)} %broadcast_in_dim.17), calls=%async_computation.19 | async-start | bytes 262144 | tf_op jit(solution)/shard_map/all_to_all | solution.py:27
  255.4 1.0 pad_maximum_fusion
  256.5 8.4 %all-to-all-done.19 = bf16[32,8,256]{2,1,0:T(8,128)(2,1)S(1)} async-done(((bf16[32,8,256]{2,1,0:T(8,128)(2,1)}), bf16[32,8,256]{2,1,0:T(8,128)(2,1)S(1)}, u32[]{:S(2)}, u32[]{:S(2)}) %all-to-all-start.19) | async-done | bytes 131104 | tf_op jit(solution)/shard_map/all_to_all | solution.py:27
  (97 shorter events, 11.6 us)
Async XLA Ops:
  0.6 16.1 %copy-start = (f32[2,16,8192]{2,1,0:T(8,128)S(1)}, f32[2,16,8192]{2,1,0:T(8,128)}, u32[]{:S(2)}) copy-start(f32[2,16,8192]{2,1,0:T(8,128)} %param.13) | copy-start | bytes 3145732
  3.1 17.1 %all-to-all-start.1 = ((f32[16,1,16]{2,1,0:T(1,128)}), f32[16,1,16]{2,1,0:T(1,128)S(1)}, u32[]{:S(2)}, u32[]{:S(2)}) async-start(f32[16,1,16]{2,1,0:T(1,128)} %all_to_all.69), calls=%async_computation.1 | async-start | bytes 16384 | tf_op jit(solution)/shard_map/all_to_all | solution.py:21
  16.8 0.8 copy-start.7
  19.3 8.0 %copy-start.2 = (bf16[2,256,128]{2,1,0:T(8,128)(2,1)S(1)}, bf16[2,256,128]{2,1,0:T(8,128)(2,1)}, u32[]{:S(2)}) copy-start(bf16[2,256,128]{2,1,0:T(8,128)(2,1)} %param.17) | copy-start | bytes 393220
  20.3 14.8 %all-to-all-start.3 = ((f32[16,1,1024]{2,1,0:T(1,128)}), f32[16,1,1024]{2,1,0:T(1,128)S(1)}, u32[]{:S(2)}, u32[]{:S(2)}) async-start(f32[16,1,1024]{2,1,0:T(1,128)} %reshape.815), calls=%async_computation.3 | async-start | bytes 131072 | tf_op jit(solution)/shard_map/all_to_all | solution.py:21
  28.1 10.3 %copy-start.16 = (f32[2,64]{1,0:T(2,128)S(1)}, f32[2,64]{1,0:T(2,128)}, u32[]{:S(2)}) copy-start(f32[2,64]{1,0:T(2,128)} %param.20) | copy-start | bytes 1540
  35.1 11.2 %all-to-all-start = ((f32[16,1,1024]{2,1,0:T(1,128)}), f32[16,1,1024]{2,1,0:T(1,128)S(1)}, u32[]{:S(2)}, u32[]{:S(2)}) async-start(f32[16,1,1024]{2,1,0:T(1,128)} %reshape.819), calls=%async_computation | async-start | bytes 131072 | tf_op jit(solution)/shard_map/all_to_all | solution.py:21
  38.5 11.2 %copy-start.17 = (f32[2,128]{1,0:T(2,128)S(1)}, f32[2,128]{1,0:T(2,128)}, u32[]{:S(2)}) copy-start(f32[2,128]{1,0:T(2,128)} %param.21) | copy-start | bytes 3076
  46.3 11.3 %all-to-all-start.2 = ((f32[16,1,1024]{2,1,0:T(1,128)}), f32[16,1,1024]{2,1,0:T(1,128)S(1)}, u32[]{:S(2)}, u32[]{:S(2)}) async-start(f32[16,1,1024]{2,1,0:T(1,128)} %reshape.817), calls=%async_computation.2 | async-start | bytes 131072 | tf_op jit(solution)/shard_map/all_to_all | solution.py:21
  50.7 23.0 %copy-start.12 = (f32[128]{0:T(128)}, f32[128]{0:T(128)S(1)}, u32[]{:S(2)}) copy-start(f32[128]{0:T(128)S(1)} %fusion.66) | copy-start | bytes 1540
  57.6 12.6 %all-to-all-start.4 = ((f32[16,16,128]{2,1,0:T(8,128)}), f32[16,16,128]{2,1,0:T(8,128)S(1)}, u32[]{:S(2)}, u32[]{:S(2)}) async-start(f32[16,16,128]{2,1,0:T(8,128)} %fusion.18), calls=%async_computation.4 | async-start | bytes 262144 | tf_op jit(solution)/shard_map/all_to_all | solution.py:21
  70.2 11.9 %all-to-all-start.5 = ((f32[16,16,128]{2,1,0:T(8,128)}), f32[16,16,128]{2,1,0:T(8,128)S(1)}, u32[]{:S(2)}, u32[]{:S(2)}) async-start(f32[16,16,128]{2,1,0:T(8,128)} %fusion.16), calls=%async_computation.5 | async-start | bytes 262144 | tf_op jit(solution)/shard_map/all_to_all | solution.py:21
  82.1 10.6 %copy-start.3 = (bf16[2,128,256]{2,1,0:T(8,128)(2,1)S(1)}, bf16[2,128,256]{2,1,0:T(8,128)(2,1)}, u32[]{:S(2)}) copy-start(bf16[2,128,256]{2,1,0:T(8,128)(2,1)} %param.22) | copy-start | bytes 393220
  114.6 4.9 %copy-start.14 = (f32[2,256]{1,0:T(2,128)S(1)}, f32[2,256]{1,0:T(2,128)}, u32[]{:S(2)}) copy-start(f32[2,256]{1,0:T(2,128)} %param.23) | copy-start | bytes 6148
  114.6 11.9 %all-to-all-start.8 = ((f32[16,1,8]{2,1,0:T(1,128)}), f32[16,1,8]{2,1,0:T(1,128)S(1)}, u32[]{:S(2)}, u32[]{:S(2)}) async-start(f32[16,1,8]{2,1,0:T(1,128)} %broadcast_in_dim.13), calls=%async_computation.8 | async-start | bytes 16384 | tf_op jit(solution)/shard_map/all_to_all | solution.py:27
  128.0 13.3 %all-to-all-start.9 = ((bf16[32,8,256]{2,1,0:T(8,128)(2,1)}), bf16[32,8,256]{2,1,0:T(8,128)(2,1)S(1)}, u32[]{:S(2)}, u32[]{:S(2)}) async-start(bf16[32,8,256]{2,1,0:T(8,128)(2,1)} %broadcast_in_dim.14), calls=%async_computation.9 | async-start | bytes 262144 | tf_op jit(solution)/shard_map/all_to_all | solution.py:27
  141.3 6.1 %copy-start.5 = (bf16[2,256,64]{1,2,0:T(8,128)(2,1)S(1)}, bf16[2,256,64]{1,2,0:T(8,128)(2,1)}, u32[]{:S(2)}) copy-start(bf16[2,256,64]{1,2,0:T(8,128)(2,1)} %param.16) | copy-start | bytes 196612
  142.1 12.3 %all-to-all-start.11 = ((f32[16,1,16]{2,1,0:T(1,128)}), f32[16,1,16]{2,1,0:T(1,128)S(1)}, u32[]{:S(2)}, u32[]{:S(2)}) async-start(f32[16,1,16]{2,1,0:T(1,128)} %bitcast.35), calls=%async_computation.11 | async-start | bytes 16384 | tf_op jit(solution)/shard_map/all_to_all | solution.py:21
  147.4 0.8 copy-start.6
  154.4 11.8 %all-to-all-start.13 = ((f32[16,1,1024]{2,1,0:T(1,128)}), f32[16,1,1024]{2,1,0:T(1,128)S(1)}, u32[]{:S(2)}, u32[]{:S(2)}) async-start(f32[16,1,1024]{2,1,0:T(1,128)} %reshape.821), calls=%async_computation.13 | async-start | bytes 131072 | tf_op jit(solution)/shard_map/all_to_all | solution.py:21
  158.6 11.1 %copy-start.1 = (bf16[2,256,128]{2,1,0:T(8,128)(2,1)S(1)}, bf16[2,256,128]{2,1,0:T(8,128)(2,1)}, u32[]{:S(2)}) copy-start(bf16[2,256,128]{2,1,0:T(8,128)(2,1)} %param.18) | copy-start | bytes 393220
  166.2 11.3 %all-to-all-start.10 = ((f32[16,1,1024]{2,1,0:T(1,128)}), f32[16,1,1024]{2,1,0:T(1,128)S(1)}, u32[]{:S(2)}, u32[]{:S(2)}) async-start(f32[16,1,1024]{2,1,0:T(1,128)} %reshape.825), calls=%async_computation.10 | async-start | bytes 131072 | tf_op jit(solution)/shard_map/all_to_all | solution.py:21
  177.5 11.3 %all-to-all-start.12 = ((f32[16,1,1024]{2,1,0:T(1,128)}), f32[16,1,1024]{2,1,0:T(1,128)S(1)}, u32[]{:S(2)}, u32[]{:S(2)}) async-start(f32[16,1,1024]{2,1,0:T(1,128)} %reshape.823), calls=%async_computation.12 | async-start | bytes 131072 | tf_op jit(solution)/shard_map/all_to_all | solution.py:21
  188.8 12.6 %all-to-all-start.14 = ((f32[16,16,128]{2,1,0:T(8,128)}), f32[16,16,128]{2,1,0:T(8,128)S(1)}, u32[]{:S(2)}, u32[]{:S(2)}) async-start(f32[16,16,128]{2,1,0:T(8,128)} %fusion.13), calls=%async_computation.14 | async-start | bytes 262144 | tf_op jit(solution)/shard_map/all_to_all | solution.py:21
  192.2 12.6 %copy-start.9 = (f32[16]{0:T(128)}, f32[16]{0:T(128)S(1)}, u32[]{:S(2)}) copy-start(f32[16]{0:T(128)S(1)} %add_rsqrt_fusion.1) | copy-start | bytes 196
  201.4 11.9 %all-to-all-start.15 = ((f32[16,16,128]{2,1,0:T(8,128)}), f32[16,16,128]{2,1,0:T(8,128)S(1)}, u32[]{:S(2)}, u32[]{:S(2)}) async-start(f32[16,16,128]{2,1,0:T(8,128)} %fusion.11), calls=%async_computation.15 | async-start | bytes 262144 | tf_op jit(solution)/shard_map/all_to_all | solution.py:21
  204.9 0.7 copy-start.8
  205.0 0.6 copy-start.13
  205.6 7.7 %copy-start.15 = (f32[128]{0:T(128)S(1)}, f32[128]{0:T(128)}, u32[]{:S(2)}) copy-start(f32[128]{0:T(128)} %get-tuple-element.16) | copy-start | bytes 1540
  213.3 0.6 copy-start.10
  213.3 11.1 %copy-start.4 = (bf16[2,128,256]{2,1,0:T(8,128)(2,1)S(1)}, bf16[2,128,256]{2,1,0:T(8,128)(2,1)}, u32[]{:S(2)}) copy-start(bf16[2,128,256]{2,1,0:T(8,128)(2,1)} %param.22) | copy-start | bytes 393220
  238.2 11.9 %all-to-all-start.18 = ((f32[16,1,8]{2,1,0:T(1,128)}), f32[16,1,8]{2,1,0:T(1,128)S(1)}, u32[]{:S(2)}, u32[]{:S(2)}) async-start(f32[16,1,8]{2,1,0:T(1,128)} %broadcast_in_dim.16), calls=%async_computation.18 | async-start | bytes 16384 | tf_op jit(solution)/shard_map/all_to_all | solution.py:27
  250.2 0.6 copy-start.11
  251.6 13.3 %all-to-all-start.19 = ((bf16[32,8,256]{2,1,0:T(8,128)(2,1)}), bf16[32,8,256]{2,1,0:T(8,128)(2,1)S(1)}, u32[]{:S(2)}, u32[]{:S(2)}) async-start(bf16[32,8,256]{2,1,0:T(8,128)(2,1)} %broadcast_in_dim.17), calls=%async_computation.19 | async-start | bytes 262144 | tf_op jit(solution)/shard_map/all_to_all | solution.py:27
where the time goes:
time: 267 us; the launch traced here: 266 us
  waiting for transfers between devices  103 us (39%)
  starting transfers between devices  71.5 us (27%)
  blocking collectives  54.7 us (20%)
  local copies, waits for them, and re-layouts  17 us (6%)
  other arithmetic  11.5 us (4%)
  matrix products  6.92 us (3%)
    all_to_all x12, waiting for transfers between devices, summed_on_arrival(): tiles = lax.all_to_all(split_up(array, dim, size), axis, 0, 0, tiled=True)  72.7 us
    all_to_all x12, starting transfers between devices, summed_on_arrival(): tiles = lax.all_to_all(split_up(array, dim, size), axis, 0, 0, tiled=True)  53.9 us
    all_to_all x2, blocking collectives, sum_at_owner(): lax.all_to_all(tiles, axis, split_axis=0, concat_axis=0, tiled=True)  33.8 us
    all_to_all x4, waiting for transfers between devices, sent_to_all(): lax.all_to_all(jnp.broadcast_to(array[None], (size, *array.shape)), axis,...  30.1 us
    all_to_all x2, blocking collectives, sent_to_all(): lax.all_to_all(jnp.broadcast_to(array[None], (size, *array.shape)), axis,...  20.9 us
    all_to_all x4, starting transfers between devices, sent_to_all(): lax.all_to_all(jnp.broadcast_to(array[None], (size, *array.shape)), axis,...  17.6 us
    unnamed x49, local copies, waits for them, and re-layouts  8.99 us
    dot_general x10, matrix products, local(): jnp.dot(normed, weights[section_index], preferred_element_type=jnp.float32)  6.59 us
  transfers between devices with their start and end apart: 16, of which 16 were waited for; matrix products, arithmetic and copies ran while one was open for 9% of the time, Pallas kernels for 0%

commit v1 on v0

v1 whole, which is shorter than its diff:
```python
import jax
import jax.numpy as jnp
from jax import lax
from jax.experimental import pallas as pl
from jax.experimental.pallas import tpu as pltpu
from jax.sharding import PartitionSpec as P

MESH = pl.DeviceIdType.MESH
D = 4096
KEY = 64
VAL = 128
NX, NY, NZ = 4, 8, 8
ROWS = 16
EPS = 1e-6
F32 = jnp.float32
BF16 = jnp.bfloat16


def ring(step, size):
    return min(step, size - step)


Y_STEPS = sorted(range(1, NY), key=lambda a: -ring(a, NY))
XZ_STEPS = sorted(
    ((a, b) for a in range(NX) for b in range(NZ) if a or b),
    key=lambda s: -ring(s[0], NX) - ring(s[1], NZ),
)


def lanes(shape):
    return lax.broadcasted_iota(jnp.int32, shape, 1)


def halves(value):
    high = value.astype(BF16)
    return high.astype(F32), (value - high.astype(F32))


def with_columns(tile, columns):
    at = lanes(tile.shape)
    for place, column in columns:
        tile = jnp.where(at == place, column, tile)
    return tile


def split_columns(stats):
    columns = []
    for i, stat in enumerate(stats):
        high, low = halves(stat)
        columns += [(KEY + 2 * i, high), (KEY + 2 * i + 1, low)]
    return columns


def stat_of(tile, i):
    return tile[:, KEY + 2 * i : KEY + 2 * i + 1] + tile[:, KEY + 2 * i + 1 : KEY + 2 * i + 2]


def kernel(
    tok_hbm, state_hbm, pre_hbm, wq_hbm, wk_hbm, wv_hbm, wg_hbm, wd_hbm, bias_hbm, hgain_hbm, wo_hbm, post_hbm,
    hid_hbm, snew_hbm,
    tok, x0, state, pre, post, bias, hgain, wq, wk, wd, w0, w1, wo,
    psend, precv, asend0, arecv0, asend1, arecv1, p1send, p1recv,
    b0, b1, csend0, csend1, crecv0, crecv1, dsend0, dsend1, d0, d1,
    ssend, srecv, hsend, hout,
    load, xsend, xrecv, phase_send, phase_recv, ready, outs,
):
    tp, dp = lax.axis_index("tp"), lax.axis_index("dp")
    z, x = tp // NX, lax.rem(tp, NX)
    y, c = dp // 2, lax.rem(dp, 2)
    other = 1 - c

    def place(dx=0, dy=0, dz=0):
        return {
            "tp": lax.rem(z + dz, NZ) * NX + lax.rem(x + dx, NX),
            "dp": lax.rem(y + dy, NY) * 2 + c,
        }

    partner = {"tp": tp, "dp": y * 2 + other}

    def fetch(source, target, i):
        copy = pltpu.make_async_copy(source, target, load.at[i])
        copy.start()
        return copy

    for a in range(NY):
        pltpu.make_async_copy(tok_hbm.at[lax.rem(y + NY - a, NY)], tok.at[:, a], load.at[0]).start()
    first = [
        fetch(pre_hbm, pre.at[c], 1),
        fetch(wq_hbm.at[0], wq.at[0], 2),
        fetch(wk_hbm.at[0], wk.at[0], 3),
        fetch(wd_hbm.at[0], wd.at[0], 4),
        fetch(wv_hbm.at[0], w0.at[:, pl.ds(0, 128)], 5),
        fetch(wg_hbm.at[0], w0.at[:, pl.ds(128, 128)], 6),
    ]
    second = [
        fetch(post_hbm, post.at[c], 7),
        fetch(wq_hbm.at[1], wq.at[1], 8),
        fetch(wk_hbm.at[1], wk.at[1], 9),
        fetch(wd_hbm.at[1], wd.at[1], 10),
        fetch(wv_hbm.at[1], w1.at[c, :, pl.ds(0, 128)], 11),
        fetch(wg_hbm.at[1], w1.at[c, :, pl.ds(128, 128)], 12),
        fetch(wo_hbm, wo.at[c], 13),
        fetch(bias_hbm, bias, 14),
        fetch(hgain_hbm, hgain, 15),
    ]
    third = [fetch(state_hbm, state, 16)]

    barrier = pltpu.get_barrier_semaphore()
    pl.semaphore_signal(barrier, inc=1, device_id=partner, device_id_type=MESH)
    for a in Y_STEPS:
        pl.semaphore_signal(barrier, inc=1, device_id=place(dy=a), device_id_type=MESH)
    for a in range(1, NZ):
        pl.semaphore_signal(barrier, inc=1, device_id=place(dz=a), device_id_type=MESH)
    for a in range(1, NX):
        pl.semaphore_signal(barrier, inc=1, device_id=place(dx=a), device_id_type=MESH)

    def join_weights(section, target):
        q, k, decay = wq[section], wk[section], wd[section]
        target[:, 256:384] = jnp.concatenate([q, k], axis=1)
        target[:, 384:512] = jnp.concatenate([decay, jnp.zeros_like(decay)], axis=1)

    pltpu.make_async_copy(tok, tok, load.at[0]).wait()
    for copy in first:
        copy.wait()
    join_weights(0, w0)

    def project_first(half):
        wide = tok[half].reshape(NY * ROWS, 256).astype(F32)
        normed = (wide * pre[c, 0:1, :]).astype(BF16)
        out = jnp.dot(normed, w0[...], preferred_element_type=F32)
        squares = jnp.sum(wide * wide, axis=1, keepdims=True)
        return jnp.concatenate(
            [out[:, :384], with_columns(out[:, 384:], split_columns([squares]))], axis=1
        )

    psend[...] = project_first(other).astype(BF16)
    own = project_first(c)
    pl.semaphore_wait(barrier, 1 + (NY - 1) + (NZ - 1) + (NX - 1))

    def send(source, target, device, i, sems):
        copy = pltpu.make_async_remote_copy(
            src_ref=source, dst_ref=target, send_sem=sems[0].at[i], recv_sem=sems[1].at[i],
            device_id=device, device_id_type=MESH,
        )
        copy.start()
        return copy

    swap = (xsend, xrecv)
    partial = send(psend, precv, partner, 0, swap)
    for a in range(1, NZ):
        pl.semaphore_signal(ready, inc=1, device_id=place(dz=a), device_id_type=MESH)

    step = (phase_send, phase_recv)

    def send_along_y(source, target, i):
        for a in Y_STEPS:
            send(source.at[a], target.at[a - 1], place(dy=NY - a), i, step)

    def arrived(ref, i):
        pltpu.make_async_copy(ref, ref, phase_recv.at[i]).wait()

    def sent(ref, i):
        pltpu.make_async_copy(ref, ref, phase_send.at[i]).wait()

    partial.wait_recv()
    own = own + precv[...].astype(F32)
    asend0[...] = own.astype(BF16).reshape(NY, ROWS, 512)
    send_along_y(asend0, arecv0, 0)
    own0 = own[:ROWS]

    for copy in second:
        copy.wait()
    join_weights(1, w1.at[c])
    exchanged = [
        send(tok.at[other], x0.at[c], partner, 1, swap),
        send(pre.at[c], pre.at[c], partner, 2, swap),
        send(post.at[c], post.at[c], partner, 3, swap),
        send(wo.at[c], wo.at[c], partner, 4, swap),
        send(w1.at[c], w1.at[c], partner, 5, swap),
    ]
    x0[c] = tok[c]
    for copy in third:
        copy.wait()

    def summed(own_rows, ref):
        total = own_rows
        for i in range(ref.shape[0]):
            total = total + ref[i].astype(F32)
        return total

    lane = lanes((ROWS, 128))
    half_sum = (
        lax.broadcasted_iota(jnp.int32, (128, 128), 0) // KEY == lax.rem(lanes((128, 128)), 2)
    ).astype(F32).astype(BF16)

    def attend(section, proj):
        values, gate = proj[:, 0:128], proj[:, 128:256]
        query = proj[:, 256:320].astype(BF16).astype(F32)
        key = proj[:, 320:384].astype(BF16).astype(F32)
        pre_decay = proj[:, 384:448] + bias[section : section + 1, :]
        log_sigmoid = jnp.minimum(pre_decay, 0.0) - jnp.log(1.0 + jnp.exp(-jnp.abs(pre_decay)))
        decay = jnp.exp(log_sigmoid / 16.0)
        faded = query * decay
        faded2 = jnp.concatenate([faded, faded], axis=1)
        terms = jnp.concatenate(
            [state[section, :, 128 * j : 128 * (j + 1)] * faded2 for j in range(KEY)], axis=0
        )
        high = terms.astype(BF16)
        low = (terms - high.astype(F32)).astype(BF16)
        sums = jnp.dot(high, half_sum, preferred_element_type=F32) + jnp.dot(
            low, half_sum, preferred_element_type=F32
        )
        old_part = jnp.zeros((ROWS, 128), F32)
        for j in range(KEY):
            old_part = jnp.where(lane // 2 == j, sums[ROWS * j : ROWS * (j + 1)], old_part)
        readout = (old_part + values * jnp.sum(query * key, axis=1, keepdims=True)) * KEY**-0.5
        mean = jnp.mean(readout * readout, axis=1, keepdims=True)
        gated = gate / (1.0 + jnp.exp(-gate))
        mixed = readout * lax.rsqrt(mean + EPS) * hgain[section : section + 1, :] * gated
        return mixed.astype(BF16), (values, key, decay)

    def update_state(section, parts):
        values, key, decay = parts
        decay2 = jnp.concatenate([decay, decay], axis=1)
        key2 = jnp.concatenate([key, key], axis=1)
        for j in range(KEY):
            value = jnp.where(lane < KEY, values[:, 2 * j : 2 * j + 1], values[:, 2 * j + 1 : 2 * j + 2])
            tile = pl.ds(128 * j, 128)
            state[section, :, tile] = decay2 * state[section, :, tile] + key2 * value
        copy = pltpu.make_async_copy(state.at[section], snew_hbm.at[section], outs.at[section])
        copy.start()
        return copy

    def send_mixed(mixed, b, i):
        b[0] = mixed
        for a in Y_STEPS:
            send(b.at[0], b.at[a], place(dy=a), i, step)

    def project_out(section, b, csend):
        gathered = b[...].reshape(NY * ROWS, 128)
        for half in range(2):
            out = jnp.dot(gathered, wo[half, section], preferred_element_type=F32).astype(BF16)
            for zz in range(NZ):
                for part in range(2):
                    csend[zz * NX + half * 2 + part] = out[ROWS * zz : ROWS * (zz + 1), 128 * part : 128 * (part + 1)]

    def send_sums(csend, crecv, i):
        for n, (a, b) in enumerate(XZ_STEPS):
            block = lax.rem(z + b, NZ) * NX + lax.rem(x + a, NX)
            send(csend.at[block], crecv.at[n], place(dx=a, dz=b), i, step)

    def send_rows(rows, dsend, d, i):
        mine = x * NZ + z
        dsend[...] = rows
        d[mine] = rows
        for a, b in XZ_STEPS:
            send(dsend, d.at[mine], place(dx=a, dz=b), i, step)

    arrived(arecv0, 0)
    total0 = summed(own0, arecv0)
    squares0 = stat_of(total0[:, 384:], 0)
    scale0 = lax.rsqrt(squares0 / D + EPS)
    mixed, parts = attend(0, total0[:, :448] * scale0)
    send_mixed(mixed, b0, 1)
    wrote = [update_state(0, parts)]

    for copy in exchanged:
        copy.wait_recv()

    def project_tokens():
        out = None
        for half in range(2):
            wide = x0[half].reshape(NY * ROWS, 256).astype(F32)
            normed = (wide * pre[half, 1:2, :]).astype(BF16)
            term = jnp.dot(normed, w1[half], preferred_element_type=F32)
            out = term if out is None else out + term
        return out

    from_tokens = project_tokens()
    p1send[...] = from_tokens.astype(BF16).reshape(NY, ROWS, 512)
    own_tokens = from_tokens[:ROWS]

    arrived(b0.at[pl.ds(1, NY - 1)], 1)
    project_out(0, b0, csend0)
    pl.semaphore_wait(ready, NZ - 1)
    send_sums(csend0, crecv0, 2)
    send_along_y(p1send, p1recv, 4)
    arrived(crecv0, 2)
    send_rows(summed(csend0[z * NX + x].astype(F32), crecv0).astype(BF16), dsend0, d0, 3)
    arrived(p1recv, 4)
    total_tokens = summed(own_tokens, p1recv)

    arrived(d0.at[pl.ds(0, NX * NZ - 1)], 3)
    out = jnp.zeros((NY * ROWS, 512), F32)
    squares_out = cross = squares_step = jnp.zeros((NY * ROWS, 1), F32)
    for half in range(2):
        rows = [
            d0[pl.ds(NZ * (2 * half + part), NZ)].reshape(NZ * ROWS, 128).astype(F32) for part in range(2)
        ]
        rows = jnp.concatenate(rows, axis=1)
        moved = rows * post[half, 0:1, :]
        wide = x0[half].reshape(NY * ROWS, 256).astype(F32)
        squares_out += jnp.sum(rows * rows, axis=1, keepdims=True)
        cross += jnp.sum(wide * moved, axis=1, keepdims=True)
        squares_step += jnp.sum(moved * moved, axis=1, keepdims=True)
        normed = (moved * pre[half, 1:2, :]).astype(BF16)
        out += jnp.dot(normed, w1[half], preferred_element_type=F32)
    own = jnp.concatenate(
        [out[:, :384], with_columns(out[:, 384:], split_columns([squares_out, cross, squares_step]))], axis=1
    )
    asend1[...] = own.astype(BF16).reshape(NY, ROWS, 512)
    send_along_y(asend1, arecv1, 5)
    own1 = own[:ROWS]
    arrived(arecv1, 5)
    total1 = summed(own1, arecv1)
    tail = total1[:, 384:]
    step_scale = lax.rsqrt(stat_of(tail, 0) / D + EPS)
    squares1 = squares0 + step_scale * (2.0 * stat_of(tail, 1) + step_scale * stat_of(tail, 2))
    scale1 = lax.rsqrt(jnp.maximum(squares1, 0.0) / D + EPS)
    mixed, parts = attend(1, (total_tokens[:, :448] + step_scale * total1[:, :448]) * scale1)
    send_mixed(mixed, b1, 6)
    wrote.append(update_state(1, parts))
    arrived(b1.at[pl.ds(1, NY - 1)], 6)
    project_out(1, b1, csend1)
    send_sums(csend1, crecv1, 7)
    arrived(crecv1, 7)
    send_rows(summed(csend1[z * NX + x].astype(F32), crecv1).astype(BF16), dsend1, d1, 8)
    arrived(d1.at[pl.ds(0, NX * NZ - 1)], 8)

    squares_last = jnp.zeros((NY * ROWS, 1), F32)
    for part in range(NX):
        rows = d1[pl.ds(NZ * part, NZ)].reshape(NZ * ROWS, 128).astype(F32)
        squares_last += jnp.sum(rows * rows, axis=1, keepdims=True)
    tile = jnp.zeros((ROWS, 128), F32)
    for a in range(NY):
        at = lax.rem(y + NY - a, NY)
        tile = jnp.where(lane == at, squares_last[ROWS * a : ROWS * (a + 1)], tile)
        tile = jnp.where(lane == NY + at, squares_out[ROWS * a : ROWS * (a + 1)], tile)
    ssend[...] = tile
    for a in Y_STEPS:
        send(ssend, srecv.at[a - 1], place(dy=a), 9, step)
    arrived(srecv, 9)
    scales = lax.rsqrt(summed(tile, srecv) / D + EPS)

    def finish(half, target):
        for a in range(NY):
            at = lax.rem(y + NY - a, NY)
            last = jnp.sum(jnp.where(lane == at, scales, 0.0), axis=1, keepdims=True)
            before = jnp.sum(jnp.where(lane == NY + at, scales, 0.0), axis=1, keepdims=True)
            for part in range(2):
                cols = pl.ds(128 * part, 128)
                slot = NZ * (2 * half + part) + a
                gain = post[half, :, cols]
                value = (
                    x0[half, a, :, cols].astype(F32)
                    + d0[slot].astype(F32) * before * gain[0:1]
                    + d1[slot].astype(F32) * last * gain[1:2]
                )
                target(at)[:, cols] = value.astype(BF16)

    finish(other, lambda at: hsend.at[at])
    result = send(hsend, hout.at[:, c], partner, 6, swap)
    finish(c, lambda at: hout.at[at, c])
    result.wait_recv()
    copy = pltpu.make_async_copy(hout, hid_hbm, outs.at[2])
    copy.start()
    wrote.append(copy)

    partial.wait_send()
    result.wait_send()
    for copy in exchanged:
        copy.wait_send()
    for ref, i in (
        (arecv0, 0), (arecv1, 5), (p1recv, 4), (b0.at[pl.ds(1, NY - 1)], 1), (b1.at[pl.ds(1, NY - 1)], 6),
        (crecv0, 2), (crecv1, 7), (d0.at[pl.ds(0, NX * NZ - 1)], 3), (d1.at[pl.ds(0, NX * NZ - 1)], 8), (srecv, 9),
    ):
        sent(ref, i)
    for copy in wrote:
        copy.wait()


def local(tokens, recurrent_state, pre_gain, w_query, w_key, w_value, w_gate, w_decay, decay_bias, head_gain, w_out, post_gain):
    vmem = pltpu.VMEM
    dma = pltpu.SemaphoreType.DMA
    blocks = NX * NZ
    hidden, state = pl.pallas_call(
        kernel,
        out_shape=(
            jax.ShapeDtypeStruct((NY, 2, ROWS, 256), BF16),
            jax.ShapeDtypeStruct((2, ROWS, VAL * KEY), F32),
        ),
        in_specs=[pl.BlockSpec(memory_space=pl.ANY)] * 12,
        out_specs=[pl.BlockSpec(memory_space=pl.ANY)] * 2,
        scratch_shapes=[
            vmem((2, NY, ROWS, 256), BF16),
            vmem((2, NY, ROWS, 256), BF16),
            vmem((2, ROWS, VAL * KEY), F32),
            vmem((2, 2, 256), F32),
            vmem((2, 2, 256), F32),
            vmem((2, KEY), F32),
            vmem((2, VAL), F32),
            vmem((2, 256, KEY), BF16),
            vmem((2, 256, KEY), BF16),
            vmem((2, 256, KEY), BF16),
            vmem((256, 512), BF16),
            vmem((2, 256, 512), BF16),
            vmem((2, 2, 128, 256), BF16),
            vmem((NY * ROWS, 512), BF16),
            vmem((NY * ROWS, 512), BF16),
            vmem((NY, ROWS, 512), BF16),
            vmem((NY - 1, ROWS, 512), BF16),
            vmem((NY, ROWS, 512), BF16),
            vmem((NY - 1, ROWS, 512), BF16),
            vmem((NY, ROWS, 512), BF16),
            vmem((NY - 1, ROWS, 512), BF16),
            vmem((NY, ROWS, 128), BF16),
            vmem((NY, ROWS, 128), BF16),
            vmem((blocks, ROWS, 128), BF16),
            vmem((blocks, ROWS, 128), BF16),
            vmem((blocks - 1, ROWS, 128), BF16),
            vmem((blocks - 1, ROWS, 128), BF16),
            vmem((ROWS, 128), BF16),
            vmem((ROWS, 128), BF16),
            vmem((blocks, ROWS, 128), BF16),
            vmem((blocks, ROWS, 128), BF16),
            vmem((ROWS, 128), F32),
            vmem((NY - 1, ROWS, 128), F32),
            vmem((NY, ROWS, 256), BF16),
            vmem((NY, 2, ROWS, 256), BF16),
            dma((17,)),
            dma((7,)),
            dma((7,)),
            dma((10,)),
            dma((10,)),
            pltpu.SemaphoreType.REGULAR,
            dma((3,)),
        ],
        compiler_params=pltpu.CompilerParams(
            collective_id=0, has_side_effects=True, vmem_limit_bytes=32 * 1024 * 1024
        ),
    )(
        tokens.reshape(NY, 2, ROWS, 256), recurrent_state, pre_gain, w_query, w_key, w_value, w_gate, w_decay,
        decay_bias, head_gain, w_out, post_gain,
    )
    return hidden.reshape(NY * 2 * ROWS, 256), state


def solution(mesh):
    in_specs = (
        P(None, "dp"), P(None, "dp", "tp"), P(None, "dp"), P(None, "dp", "tp"), P(None, "dp", "tp"),
        P(None, "dp", "tp"), P(None, "dp", "tp"), P(None, "dp", "tp"), P(None, "tp"), P(), P(None, "tp", "dp"),
        P(None, "dp"),
    )
    out_specs = (P(None, "dp"), P(None, "dp", "tp"))
    return jax.shard_map(local, mesh=mesh, in_specs=in_specs, out_specs=out_specs, check_vma=False)
```

time: 267 us -> 76.7 us (0.29)
  waiting for transfers between devices: 103 us -> 0 us
  starting transfers between devices: 71.5 us -> 0 us
  Pallas kernels: 0 us -> 69.8 us
  blocking collectives: 54.7 us -> 0 us
  other arithmetic: 11.5 us -> 0 us
  local copies, waits for them, and re-layouts: 17 us -> 5.92 us
  matrix products: 6.92 us -> 0 us
    all_to_all x16 -> x0, waiting for transfers between devices: 103 us -> none  [the longest x12 72.7 us: summed_on_arrival(): tiles = lax.all_to_all(split_up(array, dim, size), axis, 0, 0, tiled=True)]
    all_to_all x16 -> x0, starting transfers between devices: 71.5 us -> none  [the longest x12 53.9 us: summed_on_arrival(): tiles = lax.all_to_all(split_up(array, dim, size), axis, 0, 0, tiled=True)]
    pallas_call x0 -> x1, Pallas kernels: none -> 69.8 us  [local(): pl.pallas_call(kernel, out_shape=(jax.ShapeDtypeStruct((NY, 2, ROWS, 256)...]
    all_to_all x4 -> x0, blocking collectives: 54.7 us -> none  [the longest x2 33.8 us: sum_at_owner(): lax.all_to_all(tiles, axis, split_axis=0, concat_axis=0, tiled=True)]
    dot_general x12 -> x0, matrix products: 6.92 us -> none  [the longest x10 6.59 us: local(): jnp.dot(normed, weights[section_index], preferred_element_type=jnp.float32)]
    all_to_all x6 -> x0, other arithmetic: 5.05 us -> none  [summed_on_arrival(): tiles = lax.all_to_all(split_up(array, dim, size), axis, 0, 0, tiled=True)]
    reduce_sum x24 -> x0, other arithmetic: 3.4 us -> none  [the longest x2 1.39 us: local(): readout = jnp.sum(query_cols * new_state, axis=2) * KEY ** (-0.5)]
    unnamed x49 -> x23, local copies, waits for them, and re-layouts: 8.99 us -> 5.92 us
  transfers between devices with their start and end apart: 16 -> 0, of which waited for: 16 -> 0; matrix products, arithmetic and copies ran while one was open for 9% -> 0% of each run, Pallas kernels for 0% -> 0%
where the time goes in v1:
time: 76.7 us; the launch traced here: 76.5 us
  Pallas kernels  69.8 us (91%)
  local copies, waits for them, and re-layouts  5.92 us (8%)
  between operations  0.79 us (1%)
    pallas_call x1, Pallas kernels, local(): pl.pallas_call(kernel, out_shape=(jax.ShapeDtypeStruct((NY, 2, ROWS, 256)...  69.8 us
    unnamed x23, local copies, waits for them, and re-layouts  5.92 us

profile of v1, /device:TPU:1, one launch (start us, length us, event | category | flops | bytes accessed | tf_op | source)
XLA Modules:
  0.0 76.5 jit_solution(15622657284302922362)
XLA Ops:
  0.6 0.0 copy-start.4
  0.6 0.0 copy-start.5
  0.7 0.0 copy-start.6
  0.7 0.0 copy-start.7
  0.7 0.0 copy-start.8
  0.7 1.0 %copy.14.wq_hbm = bf16[2,256,64]{2,1,0:T(8,128)(2,1)S(1)} copy(bf16[2,256,64]{1,2,0:T(8,128)(2,1)} %param.15) | data formatting | bytes 131072 | tf_op args[3]
  1.7 0.0 copy-start.2
  1.7 0.0 copy-start.3
  1.7 1.0 %copy.15.wk_hbm = bf16[2,256,64]{2,1,0:T(8,128)(2,1)S(1)} copy(bf16[2,256,64]{1,2,0:T(8,128)(2,1)} %param.16) | data formatting | bytes 131072 | tf_op args[4]
  2.8 0.0 copy-start.1
  2.8 1.0 %copy.16.wd_hbm = bf16[2,256,64]{2,1,0:T(8,128)(2,1)S(1)} copy(bf16[2,256,64]{1,2,0:T(8,128)(2,1)} %param.19) | data formatting | bytes 131072 | tf_op args[7]
  3.8 0.0 copy-done.4
  3.8 0.0 copy-done.5
  3.8 0.0 copy-done.6
  3.8 0.0 copy-done.7
  3.8 0.0 copy-done.8
  3.8 0.0 copy-done.2
  3.8 0.0 copy-done.3
  3.8 0.0 copy-done.1
  3.8 0.0 copy-start
  3.9 1.2 %copy-done = f32[2,16,8192]{2,1,0:T(8,128)S(1)} copy-done((f32[2,16,8192]{2,1,0:T(8,128)S(1)}, f32[2,16,8192]{2,1,0:T(8,128)}, u32[]{:S(2)}) %copy-start) | copy-done | bytes 1048600
  5.1 69.8 %shard_map.131 = (bf16[8,2,16,256]{3,2,1,0:T(8,128)(2,1)S(1)}, f32[2,16,8192]{2,1,0:T(8,128)S(1)}) custom-call(bf16[8,2,16,256]{3,2,1,0:T(8,128)(2,1)S(1)} %bitcast.2, f32[2,16,8192]{2,1,0:T(8,128)S(1)} %copy-done, f32[2,256]{1,0:T(2,128)S(1)} %copy-done.5, bf16[2,256,64]{2,1,0:T(8,128)(2,1)S(1)} %copy.14.wq_hbm, bf16[2,256,64]{2,1,0:T(8,128)(2,1)S(1)} %copy.15.wk_hbm, ...), custom_call_target="tpu_custom_call" | custom-call | tf_op jit(solution)/shard_map/pallas_call | solution.py:386
  74.9 0.7 copy.19
  75.6 1.0 %copy.20 = f32[2,16,8192]{2,1,0:T(8,128)} copy(f32[2,16,8192]{2,1,0:T(8,128)S(1)} %get-tuple-element.9) | data formatting | bytes 2097152
Async XLA Ops:
  0.6 3.1 %copy-start.4 = (bf16[2,128,256]{2,1,0:T(8,128)(2,1)S(1)}, bf16[2,128,256]{2,1,0:T(8,128)(2,1)}, u32[]{:S(2)}) copy-start(bf16[2,128,256]{2,1,0:T(8,128)(2,1)} %wo_hbm.1) | copy-start | bytes 393220
  0.6 3.1 %copy-start.5 = (f32[2,256]{1,0:T(2,128)S(1)}, f32[2,256]{1,0:T(2,128)}, u32[]{:S(2)}) copy-start(f32[2,256]{1,0:T(2,128)} %pre_hbm.1) | copy-start | bytes 6148
  0.7 3.1 %copy-start.6 = (f32[2,256]{1,0:T(2,128)S(1)}, f32[2,256]{1,0:T(2,128)}, u32[]{:S(2)}) copy-start(f32[2,256]{1,0:T(2,128)} %post_hbm.1) | copy-start | bytes 6148
  0.7 3.1 %copy-start.7 = (f32[2,64]{1,0:T(2,128)S(1)}, f32[2,64]{1,0:T(2,128)}, u32[]{:S(2)}) copy-start(f32[2,64]{1,0:T(2,128)} %bias_hbm.1) | copy-start | bytes 1540
  0.7 3.1 %copy-start.8 = (f32[2,128]{1,0:T(2,128)S(1)}, f32[2,128]{1,0:T(2,128)}, u32[]{:S(2)}) copy-start(f32[2,128]{1,0:T(2,128)} %hgain_hbm.1) | copy-start | bytes 3076
  1.7 2.1 %copy-start.2 = (bf16[2,256,128]{2,1,0:T(8,128)(2,1)S(1)}, bf16[2,256,128]{2,1,0:T(8,128)(2,1)}, u32[]{:S(2)}) copy-start(bf16[2,256,128]{2,1,0:T(8,128)(2,1)} %wv_hbm.1) | copy-start | bytes 393220
  1.7 2.1 %copy-start.3 = (bf16[2,256,128]{2,1,0:T(8,128)(2,1)S(1)}, bf16[2,256,128]{2,1,0:T(8,128)(2,1)}, u32[]{:S(2)}) copy-start(bf16[2,256,128]{2,1,0:T(8,128)(2,1)} %wg_hbm.1) | copy-start | bytes 393220
  2.8 1.1 %copy-start.1 = (bf16[256,256]{1,0:T(8,128)(2,1)S(1)}, bf16[256,256]{1,0:T(8,128)(2,1)}, u32[]{:S(2)}) copy-start(bf16[256,256]{1,0:T(8,128)(2,1)} %param.12) | copy-start | bytes 393220
  3.8 1.2 %copy-start = (f32[2,16,8192]{2,1,0:T(8,128)S(1)}, f32[2,16,8192]{2,1,0:T(8,128)}, u32[]{:S(2)}) copy-start(f32[2,16,8192]{2,1,0:T(8,128)} %state_hbm.1) | copy-start | bytes 3145732

commit v2 on v1

--- a/solution.py
+++ b/solution.py
@@ -58,10 +58,10 @@
 def kernel(
     tok_hbm, state_hbm, pre_hbm, wq_hbm, wk_hbm, wv_hbm, wg_hbm, wd_hbm, bias_hbm, hgain_hbm, wo_hbm, post_hbm,
     hid_hbm, snew_hbm,
-    tok, x0, state, pre, post, bias, hgain, wq, wk, wd, w0, w1, wo,
+    tok, x0, state, pre, post, bias, hgain, w0, w1, wo0, wo1,
     psend, precv, asend0, arecv0, asend1, arecv1, p1send, p1recv,
-    b0, b1, csend0, csend1, crecv0, crecv1, dsend0, dsend1, d0, d1,
-    ssend, srecv, hsend, hout,
+    b0, csend0, csend1, crecv0, crecv1, dsend0, dsend1, d0, d1, dpart,
+    ssend, srecv, base, esend, erecv, hout,
     load, xsend, xrecv, phase_send, phase_recv, ready, outs,
 ):
     tp, dp = lax.axis_index("tp"), lax.axis_index("dp")
@@ -82,24 +82,35 @@
         copy.start()
         return copy
 
+    def fetch_weights(section, target, i):
+        return [
+            fetch(wv_hbm.at[section], target.at[0, :, pl.ds(0, 128)], i),
+            fetch(wg_hbm.at[section], target.at[0, :, pl.ds(128, 128)], i + 1),
+            fetch(wq_hbm.at[section], target.at[1, pl.ds(0, KEY)], i + 2),
+            fetch(wk_hbm.at[section], target.at[1, pl.ds(KEY, KEY)], i + 3),
+            fetch(wd_hbm.at[section], target.at[1, pl.ds(2 * KEY, KEY)], i + 4),
+        ]
+
+    def project(rows, weights):
+        return jnp.concatenate(
+            [
+                jnp.dot(rows, weights[0], preferred_element_type=F32),
+                lax.dot_general(rows, weights[1], (((1,), (1,)), ((), ())), preferred_element_type=F32),
+            ],
+            axis=1,
+        )
+
     for a in range(NY):
         pltpu.make_async_copy(tok_hbm.at[lax.rem(y + NY - a, NY)], tok.at[:, a], load.at[0]).start()
     first = [
         fetch(pre_hbm, pre.at[c], 1),
-        fetch(wq_hbm.at[0], wq.at[0], 2),
-        fetch(wk_hbm.at[0], wk.at[0], 3),
-        fetch(wd_hbm.at[0], wd.at[0], 4),
-        fetch(wv_hbm.at[0], w0.at[:, pl.ds(0, 128)], 5),
-        fetch(wg_hbm.at[0], w0.at[:, pl.ds(128, 128)], 6),
+        *fetch_weights(0, w0, 2),
     ]
     second = [
         fetch(post_hbm, post.at[c], 7),
-        fetch(wq_hbm.at[1], wq.at[1], 8),
-        fetch(wk_hbm.at[1], wk.at[1], 9),
-        fetch(wd_hbm.at[1], wd.at[1], 10),
-        fetch(wv_hbm.at[1], w1.at[c, :, pl.ds(0, 128)], 11),
-        fetch(wg_hbm.at[1], w1.at[c, :, pl.ds(128, 128)], 12),
-        fetch(wo_hbm, wo.at[c], 13),
+        *fetch_weights(1, w1.at[c], 8),
+        fetch(wo_hbm.at[0], wo0.at[c], 13),
+        fetch(wo_hbm.at[1], wo1.at[0, c], 17),
         fetch(bias_hbm, bias, 14),
         fetch(hgain_hbm, hgain, 15),
     ]
@@ -114,20 +125,15 @@
     for a in range(1, NX):
         pl.semaphore_signal(barrier, inc=1, device_id=place(dx=a), device_id_type=MESH)
 
-    def join_weights(section, target):
-        q, k, decay = wq[section], wk[section], wd[section]
-        target[:, 256:384] = jnp.concatenate([q, k], axis=1)
-        target[:, 384:512] = jnp.concatenate([decay, jnp.zeros_like(decay)], axis=1)
-
     pltpu.make_async_copy(tok, tok, load.at[0]).wait()
     for copy in first:
         copy.wait()
-    join_weights(0, w0)
+    w0[1, 3 * KEY :] = jnp.zeros((KEY, 256), BF16)
 
     def project_first(half):
         wide = tok[half].reshape(NY * ROWS, 256).astype(F32)
         normed = (wide * pre[c, 0:1, :]).astype(BF16)
-        out = jnp.dot(normed, w0[...], preferred_element_type=F32)
+        out = project(normed, w0)
         squares = jnp.sum(wide * wide, axis=1, keepdims=True)
         return jnp.concatenate(
             [out[:, :384], with_columns(out[:, 384:], split_columns([squares]))], axis=1
@@ -170,12 +176,13 @@
 
     for copy in second:
         copy.wait()
-    join_weights(1, w1.at[c])
+    w1[c, 1, 3 * KEY :] = jnp.zeros((KEY, 256), BF16)
     exchanged = [
         send(tok.at[other], x0.at[c], partner, 1, swap),
         send(pre.at[c], pre.at[c], partner, 2, swap),
         send(post.at[c], post.at[c], partner, 3, swap),
-        send(wo.at[c], wo.at[c], partner, 4, swap),
+        send(wo0.at[c], wo0.at[c], partner, 4, swap),
+        send(wo1.at[0, c], wo1.at[0, c], partner, 6, swap),
         send(w1.at[c], w1.at[c], partner, 5, swap),
     ]
     x0[c] = tok[c]
@@ -236,13 +243,20 @@
         for a in Y_STEPS:
             send(b.at[0], b.at[a], place(dy=a), i, step)
 
-    def project_out(section, b, csend):
+    def project_out_here(b, csend):
         gathered = b[...].reshape(NY * ROWS, 128)
         for half in range(2):
-            out = jnp.dot(gathered, wo[half, section], preferred_element_type=F32).astype(BF16)
+            out = jnp.dot(gathered, wo0[half], preferred_element_type=F32).astype(BF16)
             for zz in range(NZ):
                 for part in range(2):
                     csend[zz * NX + half * 2 + part] = out[ROWS * zz : ROWS * (zz + 1), 128 * part : 128 * (part + 1)]
+
+    def project_out_all(mixed, csend):
+        for back in range(NY):
+            for half in range(2):
+                out = jnp.dot(mixed, wo1[back, half], preferred_element_type=F32).astype(BF16)
+                for part in range(2):
+                    csend[back * NX + half * 2 + part] = out[:, 128 * part : 128 * (part + 1)]
 
     def send_sums(csend, crecv, i):
         for n, (a, b) in enumerate(XZ_STEPS):
@@ -272,7 +286,7 @@
         for half in range(2):
             wide = x0[half].reshape(NY * ROWS, 256).astype(F32)
             normed = (wide * pre[half, 1:2, :]).astype(BF16)
-            term = jnp.dot(normed, w1[half], preferred_element_type=F32)
+            term = project(normed, w1.at[half])
             out = term if out is None else out + term
         return out
 
@@ -281,16 +295,20 @@
     own_tokens = from_tokens[:ROWS]
 
     arrived(b0.at[pl.ds(1, NY - 1)], 1)
-    project_out(0, b0, csend0)
+    project_out_here(b0, csend0)
     pl.semaphore_wait(ready, NZ - 1)
     send_sums(csend0, crecv0, 2)
     send_along_y(p1send, p1recv, 4)
+    for a in Y_STEPS:
+        send(wo1.at[0, c], wo1.at[a, c], place(dy=a), 8, step)
     arrived(crecv0, 2)
     send_rows(summed(csend0[z * NX + x].astype(F32), crecv0).astype(BF16), dsend0, d0, 3)
     arrived(p1recv, 4)
     total_tokens = summed(own_tokens, p1recv)
 
     arrived(d0.at[pl.ds(0, NX * NZ - 1)], 3)
+    half_rows = 2 * NZ
+    given = [send(d0.at[pl.ds(half_rows * other, half_rows)], dpart, partner, 7, swap)]
     out = jnp.zeros((NY * ROWS, 512), F32)
     squares_out = cross = squares_step = jnp.zeros((NY * ROWS, 1), F32)
     for half in range(2):
@@ -304,13 +322,16 @@
         cross += jnp.sum(wide * moved, axis=1, keepdims=True)
         squares_step += jnp.sum(moved * moved, axis=1, keepdims=True)
         normed = (moved * pre[half, 1:2, :]).astype(BF16)
-        out += jnp.dot(normed, w1[half], preferred_element_type=F32)
+        out += project(normed, w1.at[half])
     own = jnp.concatenate(
         [out[:, :384], with_columns(out[:, 384:], split_columns([squares_out, cross, squares_step]))], axis=1
     )
     asend1[...] = own.astype(BF16).reshape(NY, ROWS, 512)
     send_along_y(asend1, arecv1, 5)
     own1 = own[:ROWS]
+    gathered_out = wo1.at[pl.ds(1, NY - 1), c]
+    arrived(gathered_out, 8)
+    given.append(send(gathered_out, gathered_out, partner, 8, swap))
     arrived(arecv1, 5)
     total1 = summed(own1, arecv1)
     tail = total1[:, 384:]
@@ -318,61 +339,68 @@
     squares1 = squares0 + step_scale * (2.0 * stat_of(tail, 1) + step_scale * stat_of(tail, 2))
     scale1 = lax.rsqrt(jnp.maximum(squares1, 0.0) / D + EPS)
     mixed, parts = attend(1, (total_tokens[:, :448] + step_scale * total1[:, :448]) * scale1)
-    send_mixed(mixed, b1, 6)
+    for copy in given:
+        copy.wait_recv()
+    project_out_all(mixed, csend1)
+    send_sums(csend1, crecv1, 6)
+
+    def send_over_chips(source, target, i):
+        for k in Y_STEPS + [0]:
+            for r in range(2):
+                if r == 0 and k == 0:
+                    continue
+                device = {"tp": tp, "dp": lax.rem(y + NY - k, NY) * 2 + (other if r else c)}
+                send(source(r * NY + k), target.at[r * NY + k], device, i, step)
+
+    own_scale = jnp.broadcast_to(step_scale, (ROWS, 128))
+    ssend[...] = own_scale
+    srecv[0] = own_scale
+    send_over_chips(lambda slot: ssend, srecv, 9)
     wrote.append(update_state(1, parts))
-    arrived(b1.at[pl.ds(1, NY - 1)], 6)
-    project_out(1, b1, csend1)
-    send_sums(csend1, crecv1, 7)
-    arrived(crecv1, 7)
-    send_rows(summed(csend1[z * NX + x].astype(F32), crecv1).astype(BF16), dsend1, d1, 8)
-    arrived(d1.at[pl.ds(0, NX * NZ - 1)], 8)
-
-    squares_last = jnp.zeros((NY * ROWS, 1), F32)
-    for part in range(NX):
-        rows = d1[pl.ds(NZ * part, NZ)].reshape(NZ * ROWS, 128).astype(F32)
-        squares_last += jnp.sum(rows * rows, axis=1, keepdims=True)
-    tile = jnp.zeros((ROWS, 128), F32)
-    for a in range(NY):
-        at = lax.rem(y + NY - a, NY)
-        tile = jnp.where(lane == at, squares_last[ROWS * a : ROWS * (a + 1)], tile)
-        tile = jnp.where(lane == NY + at, squares_out[ROWS * a : ROWS * (a + 1)], tile)
-    ssend[...] = tile
-    for a in Y_STEPS:
-        send(ssend, srecv.at[a - 1], place(dy=a), 9, step)
-    arrived(srecv, 9)
-    scales = lax.rsqrt(summed(tile, srecv) / D + EPS)
-
-    def finish(half, target):
-        for a in range(NY):
-            at = lax.rem(y + NY - a, NY)
-            last = jnp.sum(jnp.where(lane == at, scales, 0.0), axis=1, keepdims=True)
-            before = jnp.sum(jnp.where(lane == NY + at, scales, 0.0), axis=1, keepdims=True)
+    arrived(crecv1, 6)
+    send_rows(summed(csend1[z * NX + x].astype(F32), crecv1).astype(BF16), dsend1, d1, 7)
+
+    arrived(srecv.at[pl.ds(1, 2 * NY - 1)], 9)
+    for r in range(2):
+        for k in range(NY):
+            a = (NY - k) % NY
             for part in range(2):
                 cols = pl.ds(128 * part, 128)
-                slot = NZ * (2 * half + part) + a
-                gain = post[half, :, cols]
-                value = (
-                    x0[half, a, :, cols].astype(F32)
-                    + d0[slot].astype(F32) * before * gain[0:1]
-                    + d1[slot].astype(F32) * last * gain[1:2]
+                rows = dpart[NZ * part + a] if r else d0[half_rows * c + NZ * part + a]
+                base[r * NY + k, :, cols] = (
+                    tok[other if r else c, a, :, cols].astype(F32)
+                    + rows.astype(F32) * srecv[r * NY + k] * post[c, 0:1, cols]
                 )
-                target(at)[:, cols] = value.astype(BF16)
-
-    finish(other, lambda at: hsend.at[at])
-    result = send(hsend, hout.at[:, c], partner, 6, swap)
-    finish(c, lambda at: hout.at[at, c])
-    result.wait_recv()
+
+    arrived(d1.at[pl.ds(0, NX * NZ - 1)], 7)
+    squares_last = jnp.zeros((ROWS, 128), F32)
+    for slot in range(NX * NZ):
+        rows = d1[slot].astype(F32)
+        squares_last += rows * rows
+    last_scale = lax.rsqrt(jnp.sum(squares_last, axis=1, keepdims=True) / D + EPS)
+    for r in range(2):
+        for k in range(NY):
+            for part in range(2):
+                rows = d1[half_rows * (other if r else c) + NZ * part + k].astype(F32)
+                esend[r * NY + k, :, pl.ds(128 * part, 128)] = (rows * last_scale).astype(BF16)
+    erecv[0] = esend[0]
+    send_over_chips(lambda slot: esend.at[slot], erecv, 10)
+    arrived(erecv.at[pl.ds(1, 2 * NY - 1)], 10)
+    for r in range(2):
+        for k in range(NY):
+            value = base[r * NY + k] + erecv[r * NY + k].astype(F32) * post[c, 1:2, :]
+            hout[lax.rem(y + k, NY), other if r else c] = value.astype(BF16)
     copy = pltpu.make_async_copy(hout, hid_hbm, outs.at[2])
     copy.start()
     wrote.append(copy)
 
     partial.wait_send()
-    result.wait_send()
-    for copy in exchanged:
+    for copy in exchanged + given:
         copy.wait_send()
     for ref, i in (
-        (arecv0, 0), (arecv1, 5), (p1recv, 4), (b0.at[pl.ds(1, NY - 1)], 1), (b1.at[pl.ds(1, NY - 1)], 6),
-        (crecv0, 2), (crecv1, 7), (d0.at[pl.ds(0, NX * NZ - 1)], 3), (d1.at[pl.ds(0, NX * NZ - 1)], 8), (srecv, 9),
+        (arecv0, 0), (arecv1, 5), (p1recv, 4), (b0.at[pl.ds(1, NY - 1)], 1), (gathered_out, 8), (crecv0, 2), (crecv1, 6),
+        (d0.at[pl.ds(0, NX * NZ - 1)], 3), (d1.at[pl.ds(0, NX * NZ - 1)], 7), (srecv.at[pl.ds(1, 2 * NY - 1)], 9),
+        (erecv.at[pl.ds(1, 2 * NY - 1)], 10),
     ):
         sent(ref, i)
     for copy in wrote:
@@ -389,7 +417,7 @@
             jax.ShapeDtypeStruct((NY, 2, ROWS, 256), BF16),
             jax.ShapeDtypeStruct((2, ROWS, VAL * KEY), F32),
         ),
-        in_specs=[pl.BlockSpec(memory_space=pl.ANY)] * 12,
+        in_specs=[pl.BlockSpec(memory_space=pltpu.HBM)] * 12,
         out_specs=[pl.BlockSpec(memory_space=pl.ANY)] * 2,
         scratch_shapes=[
             vmem((2, NY, ROWS, 256), BF16),
@@ -399,12 +427,10 @@
             vmem((2, 2, 256), F32),
             vmem((2, KEY), F32),
             vmem((2, VAL), F32),
-            vmem((2, 256, KEY), BF16),
-            vmem((2, 256, KEY), BF16),
-            vmem((2, 256, KEY), BF16),
-            vmem((256, 512), BF16),
-            vmem((2, 256, 512), BF16),
-            vmem((2, 2, 128, 256), BF16),
+            vmem((2, 256, 256), BF16),
+            vmem((2, 2, 256, 256), BF16),
+            vmem((2, 128, 256), BF16),
+            vmem((NY, 2, 128, 256), BF16),
             vmem((NY * ROWS, 512), BF16),
             vmem((NY * ROWS, 512), BF16),
             vmem((NY, ROWS, 512), BF16),
@@ -414,7 +440,6 @@
             vmem((NY, ROWS, 512), BF16),
             vmem((NY - 1, ROWS, 512), BF16),
             vmem((NY, ROWS, 128), BF16),
-            vmem((NY, ROWS, 128), BF16),
             vmem((blocks, ROWS, 128), BF16),
             vmem((blocks, ROWS, 128), BF16),
             vmem((blocks - 1, ROWS, 128), BF16),
@@ -423,15 +448,18 @@
             vmem((ROWS, 128), BF16),
             vmem((blocks, ROWS, 128), BF16),
             vmem((blocks, ROWS, 128), BF16),
+            vmem((2 * NZ, ROWS, 128), BF16),
             vmem((ROWS, 128), F32),
-            vmem((NY - 1, ROWS, 128), F32),
-            vmem((NY, ROWS, 256), BF16),
+            vmem((2 * NY, ROWS, 128), F32),
+            vmem((2 * NY, ROWS, 256), F32),
+            vmem((2 * NY, ROWS, 256), BF16),
+            vmem((2 * NY, ROWS, 256), BF16),
             vmem((NY, 2, ROWS, 256), BF16),
-            dma((17,)),
-            dma((7,)),
-            dma((7,)),
-            dma((10,)),
-            dma((10,)),
+            dma((18,)),
+            dma((9,)),
+            dma((9,)),
+            dma((11,)),
+            dma((11,)),
             pltpu.SemaphoreType.REGULAR,
             dma((3,)),
         ],
@@ -439,8 +467,10 @@
             collective_id=0, has_side_effects=True, vmem_limit_bytes=32 * 1024 * 1024
         ),
     )(
-        tokens.reshape(NY, 2, ROWS, 256), recurrent_state, pre_gain, w_query, w_key, w_value, w_gate, w_decay,
-        decay_bias, head_gain, w_out, post_gain,
+        *(pltpu.with_memory_space_constraint(v, pltpu.HBM) for v in (
+        tokens.reshape(NY, 2, ROWS, 256), recurrent_state, pre_gain, jnp.swapaxes(w_query, 1, 2),
+        jnp.swapaxes(w_key, 1, 2), w_value, w_gate, jnp.swapaxes(w_decay, 1, 2),
+        decay_bias, head_gain, w_out, post_gain,))
     )
     return hidden.reshape(NY * 2 * ROWS, 256), state
 

time: 76.7 us -> 67 us (0.87)
  Pallas kernels: 69.8 us -> 64.6 us
  local copies, waits for them, and re-layouts: 5.92 us -> 1.63 us
    pallas_call x1, Pallas kernels: 69.8 us -> 64.6 us  [local(): pl.pallas_call(kernel, out_shape=(jax.ShapeDtypeStruct((NY, 2, ROWS, 256)...]
    unnamed x23 -> x2, local copies, waits for them, and re-layouts: 5.92 us -> 1.63 us
where the time goes in v2:
time: 67 us; the launch traced here: 66.9 us
  Pallas kernels  64.6 us (96%)
  local copies, waits for them, and re-layouts  1.63 us (2%)
    pallas_call x1, Pallas kernels, local(): pl.pallas_call(kernel, out_shape=(jax.ShapeDtypeStruct((NY, 2, ROWS, 256)...  64.6 us
    unnamed x2, local copies, waits for them, and re-layouts  1.63 us

profile of v2, /device:TPU:1, one launch (start us, length us, event | category | flops | bytes accessed | tf_op | source)
XLA Modules:
  0.0 66.9 jit_solution(5323516262102623842)
XLA Ops:
  0.6 64.6 %shard_map.131 = (bf16[8,2,16,256]{3,2,1,0:T(8,128)(2,1)S(1)}, f32[2,16,8192]{2,1,0:T(8,128)S(1)}) custom-call(bf16[8,2,16,256]{3,2,1,0:T(8,128)(2,1)} %bitcast.6, f32[2,16,8192]{2,1,0:T(8,128)} %state_hbm.1, f32[2,256]{1,0:T(2,128)} %pre_hbm.1, bf16[2,64,256]{2,1,0:T(8,128)(2,1)} %bitcast.7, bf16[2,64,256]{2,1,0:T(8,128)(2,1)} %bitcast.8, ...), custom_call_target="tpu_custom_call" | custom-call | tf_op jit(solution)/shard_map/pallas_call | solution.py:414
  65.3 0.7 copy.16
  65.9 1.0 %copy.17 = f32[2,16,8192]{2,1,0:T(8,128)} copy(f32[2,16,8192]{2,1,0:T(8,128)S(1)} %get-tuple-element.9) | data formatting | bytes 2097152

commit v3 on v2

--- a/solution.py
+++ b/solution.py
@@ -57,12 +57,12 @@
 
 def kernel(
     tok_hbm, state_hbm, pre_hbm, wq_hbm, wk_hbm, wv_hbm, wg_hbm, wd_hbm, bias_hbm, hgain_hbm, wo_hbm, post_hbm,
-    hid_hbm, snew_hbm,
+    hout, snew,
     tok, x0, state, pre, post, bias, hgain, w0, w1, wo0, wo1,
     psend, precv, asend0, arecv0, asend1, arecv1, p1send, p1recv,
     b0, csend0, csend1, crecv0, crecv1, dsend0, dsend1, d0, d1, dpart,
-    ssend, srecv, base, esend, erecv, hout,
-    load, xsend, xrecv, phase_send, phase_recv, ready, outs,
+    ssend, srecv, base, esend, erecv,
+    load, xsend, xrecv, phase_send, phase_recv, ready,
 ):
     tp, dp = lax.axis_index("tp"), lax.axis_index("dp")
     z, x = tp // NX, lax.rem(tp, NX)
@@ -76,6 +76,15 @@
         }
 
     partner = {"tp": tp, "dp": y * 2 + other}
+
+    barrier = pltpu.get_barrier_semaphore()
+    for a in Y_STEPS:
+        pl.semaphore_signal(barrier, inc=1, device_id=place(dy=a), device_id_type=MESH)
+    for a in range(1, NZ):
+        pl.semaphore_signal(barrier, inc=1, device_id=place(dz=a), device_id_type=MESH)
+    for a in range(1, NX):
+        pl.semaphore_signal(barrier, inc=1, device_id=place(dx=a), device_id_type=MESH)
+    pl.semaphore_signal(barrier, inc=1, device_id=partner, device_id_type=MESH)
 
     def fetch(source, target, i):
         copy = pltpu.make_async_copy(source, target, load.at[i])
@@ -115,15 +124,6 @@
         fetch(hgain_hbm, hgain, 15),
     ]
     third = [fetch(state_hbm, state, 16)]
-
-    barrier = pltpu.get_barrier_semaphore()
-    pl.semaphore_signal(barrier, inc=1, device_id=partner, device_id_type=MESH)
-    for a in Y_STEPS:
-        pl.semaphore_signal(barrier, inc=1, device_id=place(dy=a), device_id_type=MESH)
-    for a in range(1, NZ):
-        pl.semaphore_signal(barrier, inc=1, device_id=place(dz=a), device_id_type=MESH)
-    for a in range(1, NX):
-        pl.semaphore_signal(barrier, inc=1, device_id=place(dx=a), device_id_type=MESH)
 
     pltpu.make_async_copy(tok, tok, load.at[0]).wait()
     for copy in first:
@@ -233,10 +233,7 @@
         for j in range(KEY):
             value = jnp.where(lane < KEY, values[:, 2 * j : 2 * j + 1], values[:, 2 * j + 1 : 2 * j + 2])
             tile = pl.ds(128 * j, 128)
-            state[section, :, tile] = decay2 * state[section, :, tile] + key2 * value
-        copy = pltpu.make_async_copy(state.at[section], snew_hbm.at[section], outs.at[section])
-        copy.start()
-        return copy
+            snew[section, :, tile] = decay2 * state[section, :, tile] + key2 * value
 
     def send_mixed(mixed, b, i):
         b[0] = mixed
@@ -276,7 +273,7 @@
     scale0 = lax.rsqrt(squares0 / D + EPS)
     mixed, parts = attend(0, total0[:, :448] * scale0)
     send_mixed(mixed, b0, 1)
-    wrote = [update_state(0, parts)]
+    update_state(0, parts)
 
     for copy in exchanged:
         copy.wait_recv()
@@ -293,22 +290,30 @@
     from_tokens = project_tokens()
     p1send[...] = from_tokens.astype(BF16).reshape(NY, ROWS, 512)
     own_tokens = from_tokens[:ROWS]
+    send_along_y(p1send, p1recv, 4)
 
     arrived(b0.at[pl.ds(1, NY - 1)], 1)
     project_out_here(b0, csend0)
     pl.semaphore_wait(ready, NZ - 1)
     send_sums(csend0, crecv0, 2)
-    send_along_y(p1send, p1recv, 4)
-    for a in Y_STEPS:
+    for a in (2, NY - 2, 1, NY - 1):
         send(wo1.at[0, c], wo1.at[a, c], place(dy=a), 8, step)
     arrived(crecv0, 2)
     send_rows(summed(csend0[z * NX + x].astype(F32), crecv0).astype(BF16), dsend0, d0, 3)
+    arrived(wo1.at[pl.ds(0, 4), c], 8)
+    front, back = pl.ds(0, 64), pl.ds(64, 64)
+    send(wo1.at[2, c, front], wo1.at[4, c, front], place(dy=2), 11, step)
+    send(wo1.at[6, c, back], wo1.at[4, c, back], place(dy=NY - 2), 11, step)
+    send(wo1.at[2, c], wo1.at[3, c], place(dy=1), 11, step)
+    send(wo1.at[6, c], wo1.at[5, c], place(dy=NY - 1), 11, step)
+    near, far, rest = (wo1.at[pl.ds(first, count), c] for first, count in ((1, 2), (6, 2), (3, 3)))
+    given = [send(near, near, partner, 8, swap), send(far, far, partner, 9, swap)]
     arrived(p1recv, 4)
     total_tokens = summed(own_tokens, p1recv)
 
     arrived(d0.at[pl.ds(0, NX * NZ - 1)], 3)
     half_rows = 2 * NZ
-    given = [send(d0.at[pl.ds(half_rows * other, half_rows)], dpart, partner, 7, swap)]
+    given.append(send(d0.at[pl.ds(half_rows * other, half_rows)], dpart, partner, 7, swap))
     out = jnp.zeros((NY * ROWS, 512), F32)
     squares_out = cross = squares_step = jnp.zeros((NY * ROWS, 1), F32)
     for half in range(2):
@@ -329,9 +334,8 @@
     asend1[...] = own.astype(BF16).reshape(NY, ROWS, 512)
     send_along_y(asend1, arecv1, 5)
     own1 = own[:ROWS]
-    gathered_out = wo1.at[pl.ds(1, NY - 1), c]
-    arrived(gathered_out, 8)
-    given.append(send(gathered_out, gathered_out, partner, 8, swap))
+    arrived(rest, 11)
+    given.append(send(rest, rest, partner, 10, swap))
     arrived(arecv1, 5)
     total1 = summed(own1, arecv1)
     tail = total1[:, 384:]
@@ -356,7 +360,7 @@
     ssend[...] = own_scale
     srecv[0] = own_scale
     send_over_chips(lambda slot: ssend, srecv, 9)
-    wrote.append(update_state(1, parts))
+    update_state(1, parts)
     arrived(crecv1, 6)
     send_rows(summed(csend1[z * NX + x].astype(F32), crecv1).astype(BF16), dsend1, d1, 7)
 
@@ -390,20 +394,25 @@
         for k in range(NY):
             value = base[r * NY + k] + erecv[r * NY + k].astype(F32) * post[c, 1:2, :]
             hout[lax.rem(y + k, NY), other if r else c] = value.astype(BF16)
-    copy = pltpu.make_async_copy(hout, hid_hbm, outs.at[2])
-    copy.start()
-    wrote.append(copy)
-
     partial.wait_send()
     for copy in exchanged + given:
         copy.wait_send()
     for ref, i in (
-        (arecv0, 0), (arecv1, 5), (p1recv, 4), (b0.at[pl.ds(1, NY - 1)], 1), (gathered_out, 8), (crecv0, 2), (crecv1, 6),
+        (arecv0, 0), (arecv1, 5), (p1recv, 4), (b0.at[pl.ds(1, NY - 1)], 1), (wo1.at[pl.ds(0, 4), c], 8), (rest, 11), (crecv0, 2), (crecv1, 6),
         (d0.at[pl.ds(0, NX * NZ - 1)], 3), (d1.at[pl.ds(0, NX * NZ - 1)], 7), (srecv.at[pl.ds(1, 2 * NY - 1)], 9),
         (erecv.at[pl.ds(1, 2 * NY - 1)], 10),
     ):
         sent(ref, i)
-    for copy in wrote:
+
+
+def write_out(hidden, state, hidden_out, state_out, done):
+    copies = [
+        pltpu.make_async_copy(state, state_out, done.at[0]),
+        pltpu.make_async_copy(hidden, hidden_out, done.at[1]),
+    ]
+    for copy in copies:
+        copy.start()
+    for copy in copies:
         copy.wait()
 
 
@@ -418,7 +427,7 @@
             jax.ShapeDtypeStruct((2, ROWS, VAL * KEY), F32),
         ),
         in_specs=[pl.BlockSpec(memory_space=pltpu.HBM)] * 12,
-        out_specs=[pl.BlockSpec(memory_space=pl.ANY)] * 2,
+        out_specs=[pl.BlockSpec(memory_space=pltpu.VMEM)] * 2,
         scratch_shapes=[
             vmem((2, NY, ROWS, 256), BF16),
             vmem((2, NY, ROWS, 256), BF16),
@@ -454,14 +463,12 @@
             vmem((2 * NY, ROWS, 256), F32),
             vmem((2 * NY, ROWS, 256), BF16),
             vmem((2 * NY, ROWS, 256), BF16),
-            vmem((NY, 2, ROWS, 256), BF16),
             dma((18,)),
-            dma((9,)),
-            dma((9,)),
             dma((11,)),
             dma((11,)),
+            dma((12,)),
+            dma((12,)),
             pltpu.SemaphoreType.REGULAR,
-            dma((3,)),
         ],
         compiler_params=pltpu.CompilerParams(
             collective_id=0, has_side_effects=True, vmem_limit_bytes=32 * 1024 * 1024
@@ -472,6 +479,14 @@
         jnp.swapaxes(w_key, 1, 2), w_value, w_gate, jnp.swapaxes(w_decay, 1, 2),
         decay_bias, head_gain, w_out, post_gain,))
     )
+    hidden, state = pl.pallas_call(
+        write_out,
+        out_shape=(jax.ShapeDtypeStruct(hidden.shape, BF16), jax.ShapeDtypeStruct(state.shape, F32)),
+        in_specs=[pl.BlockSpec(memory_space=pl.ANY)] * 2,
+        out_specs=[pl.BlockSpec(memory_space=pl.ANY)] * 2,
+        scratch_shapes=[dma((2,))],
+        compiler_params=pltpu.CompilerParams(vmem_limit_bytes=1024 * 1024),
+    )(hidden, state)
     return hidden.reshape(NY * 2 * ROWS, 256), state
 
 

time: 67 us -> 64.4 us (0.961)
  local copies, waits for them, and re-layouts: 1.63 us -> 0 us
  Pallas kernels: 64.6 us -> 63.6 us
    pallas_call x1, Pallas kernels: 64.6 us -> 62.6 us  [local(): pl.pallas_call(kernel, out_shape=(jax.ShapeDtypeStruct((NY, 2, ROWS, 256)...]
    unnamed x2 -> x0, local copies, waits for them, and re-layouts: 1.63 us -> none
    pallas_call x0 -> x1, Pallas kernels: none -> 1.02 us  [local(): pl.pallas_call(write_out, out_shape=(jax.ShapeDtypeStruct(hidden.shape, B...]
where the time goes in v3:
time: 64.4 us; the launch traced here: 64.2 us
  Pallas kernels  63.6 us (99%)
    pallas_call x1, Pallas kernels, local(): pl.pallas_call(kernel, out_shape=(jax.ShapeDtypeStruct((NY, 2, ROWS, 256)...  62.6 us

profile of v3, /device:TPU:1, one launch (start us, length us, event | category | flops | bytes accessed | tf_op | source)
XLA Modules:
  0.0 64.2 jit_solution(3994984195097081483)
XLA Ops:
  0.6 62.6 %shard_map.131 = (bf16[8,2,16,256]{3,2,1,0:T(8,128)(2,1)S(1)}, f32[2,16,8192]{2,1,0:T(8,128)S(1)}) custom-call(bf16[8,2,16,256]{3,2,1,0:T(8,128)(2,1)} %bitcast.5, f32[2,16,8192]{2,1,0:T(8,128)} %state_hbm.1, f32[2,256]{1,0:T(2,128)} %pre_hbm.1, bf16[2,64,256]{2,1,0:T(8,128)(2,1)} %bitcast.6, bf16[2,64,256]{2,1,0:T(8,128)(2,1)} %bitcast.7, ...), custom_call_target="tpu_custom_call" | custom-call | tf_op jit(solution)/shard_map/pallas_call | solution.py:423
  63.2 1.0 %shard_map.132 = (bf16[8,2,16,256]{3,2,1,0:T(8,128)(2,1)}, f32[2,16,8192]{2,1,0:T(8,128)}) custom-call(bf16[8,2,16,256]{3,2,1,0:T(8,128)(2,1)S(1)} %get-tuple-element.6.hidden, f32[2,16,8192]{2,1,0:T(8,128)S(1)} %get-tuple-element.7.state), custom_call_target="tpu_custom_call" | custom-call | tf_op jit(solution)/shard_map/pallas_call | solution.py:482

commit v4 on v3

--- a/solution.py
+++ b/solution.py
@@ -23,7 +23,7 @@
 Y_STEPS = sorted(range(1, NY), key=lambda a: -ring(a, NY))
 XZ_STEPS = sorted(
     ((a, b) for a in range(NX) for b in range(NZ) if a or b),
-    key=lambda s: -ring(s[0], NX) - ring(s[1], NZ),
+    key=lambda s: (-ring(s[0], NX) - ring(s[1], NZ), -ring(s[0], NX)),
 )
 
 
@@ -350,7 +350,7 @@
 
     def send_over_chips(source, target, i):
         for k in Y_STEPS + [0]:
-            for r in range(2):
+            for r in (1, 0):
                 if r == 0 and k == 0:
                     continue
                 device = {"tp": tp, "dp": lax.rem(y + NY - k, NY) * 2 + (other if r else c)}

time: 64.4 us -> 64.2 us (level)
  no operation moved by 1% of the time
where the time goes in v4:
time: 64.2 us; the launch traced here: 64.1 us
  Pallas kernels  63.4 us (99%)
    pallas_call x1, Pallas kernels, local(): pl.pallas_call(kernel, out_shape=(jax.ShapeDtypeStruct((NY, 2, ROWS, 256)...  62.4 us

profile of v4, /device:TPU:1, one launch (start us, length us, event | category | flops | bytes accessed | tf_op | source)
XLA Modules:
  0.0 64.1 jit_solution(8732965523394859946)
XLA Ops:
  0.6 62.4 %shard_map.131 = (bf16[8,2,16,256]{3,2,1,0:T(8,128)(2,1)S(1)}, f32[2,16,8192]{2,1,0:T(8,128)S(1)}) custom-call(bf16[8,2,16,256]{3,2,1,0:T(8,128)(2,1)} %bitcast.5, f32[2,16,8192]{2,1,0:T(8,128)} %state_hbm.1, f32[2,256]{1,0:T(2,128)} %pre_hbm.1, bf16[2,64,256]{2,1,0:T(8,128)(2,1)} %bitcast.6, bf16[2,64,256]{2,1,0:T(8,128)(2,1)} %bitcast.7, ...), custom_call_target="tpu_custom_call" | custom-call | tf_op jit(solution)/shard_map/pallas_call | solution.py:423
  63.1 1.0 %shard_map.132 = (bf16[8,2,16,256]{3,2,1,0:T(8,128)(2,1)}, f32[2,16,8192]{2,1,0:T(8,128)}) custom-call(bf16[8,2,16,256]{3,2,1,0:T(8,128)(2,1)S(1)} %get-tuple-element.6.hidden, f32[2,16,8192]{2,1,0:T(8,128)S(1)} %get-tuple-element.7.state), custom_call_target="tpu_custom_call" | custom-call | tf_op jit(solution)/shard_map/pallas_call | solution.py:482
